TPU v7x, 256 devices: a 4x2x16 block of a 4x16x16 slice. The times are simulated.
256 devices in a mesh: grp: 2 (over y), sp: 32 (over z, core), tp: 4 (over x).
Axes of the slice: x: 4, y: 2, z: 16, core: 2. Of those that a mesh axis runs over, the one named last changes fastest.
The devices are a block of a 4x16x16 slice.
Arguments:
- queries: bfloat16 [8192, 2048], P(('grp', 'sp'), 'tp'), parts along dimension 0, may hold values from -8 to 8
- keys: bfloat16 [8192, 1024], P(('grp', 'sp'), 'tp'), parts along dimension 0, may hold values from -6 to 6
- values: bfloat16 [8192, 1024], P(('grp', 'sp'), 'tp'), parts along dimension 0, may hold values from -6 to 6
- head_bias: float32 [16], P('tp'), may hold values from -15 to -5
- documents: int32 [8192], P(('grp', 'sp')), parts along dimension 0, may hold values from 0 to 2, never falling along the last dimension, each value on 1 to 3072 neighbouring positions
- w_out: bfloat16 [2048, 2048], P('tp'), may hold values from -0.125 to 0.125
- resid: bfloat16 [8192, 2048], P(('grp', 'sp', 'tp')), parts along dimension 0, may hold values from -6 to 6
- norm_gain: float32 [2048], replicated, may hold values from 0.1 to 1.9
- expert_ids: int32 [8192, 2], P(('grp', 'sp', 'tp')), parts along dimension 0, may hold values from 0 to 31, all different within a row; in each aligned block of 32 rows (0 to 31, 32 to 63, ...) at most 4 rows name the same one
- expert_gates: float32 [8192, 2], P(('grp', 'sp', 'tp')), parts along dimension 0, may hold values from 0.1 to 0.9
- w_gate: bfloat16 [32, 2048, 3072], P('sp', None, 'tp'), may hold values from -0.125 to 0.125
- w_up: bfloat16 [32, 2048, 3072], P('sp', None, 'tp'), may hold values from -0.125 to 0.125
- w_down: bfloat16 [32, 3072, 2048], P('sp', 'tp'), may hold values from -0.109375 to 0.109375
Outputs:
- layer_out: bfloat16 [8192, 2048], P(('grp', 'sp', 'tp')), parts along dimension 0
There are 2 independent parts, one for each index of `grp`. A program takes and returns all parts, laid end to end along the dimension named above; an argument that names none is the same for every part. Nothing has to cross between parts.
Inputs may be any that keep to these rules, and one draw needn't show every extreme that they name: Document numbers never fall along the sequence; each of the 3 documents holds at least one position and the longest exactly 3072 positions. `expert_ids`: each position names 2 different experts. Among the 32 positions of one device (aligned blocks of 32 rows) no expert is named more than 4 times, and in some block some expert exactly 4 times.
All inputs are finite; a program needn't handle non-finite values.
Results may differ from a plain program's by a relative error of at most 0.012.
Values may be sent and summed in bfloat16 or wider, within the bound.
A program may use at most 64 MiB of HBM per device.

v0:
```python
import jax
import jax.numpy as jnp
from jax import lax
from jax.sharding import Mesh
from jax.sharding import PartitionSpec as P

D = 2048
HEADS = 16
KV_HEADS = 8
DH = 128
TOPK = 2
SP = ("sp_0", "sp_1")
GRP_SP = ("grp", "sp_0", "sp_1")
GRP_SP_TP = ("grp", "sp_0", "sp_1", "tp")


def sent_together(arrays, axis, dim, along):
    widths = [a.shape[along] for a in arrays]
    both = jnp.concatenate(arrays, axis=along)
    filled = lax.all_gather(both, axis, axis=dim, tiled=True)
    return tuple(jnp.split(filled, [sum(widths[:k]) for k in range(1, len(widths))], axis=along))


def in_blocks(shard, dim, peers):
    before, after = (shard.shape[:dim], shard.shape[dim + 1 :])
    return jnp.moveaxis(shard.reshape(*before, peers, -1, *after), dim, 0)


def summed_on_arrival(shard, axis, dim):
    blocks = in_blocks(shard, dim, lax.axis_size(axis))
    arrived = lax.all_to_all(blocks, axis, split_axis=0, concat_axis=0, tiled=True)
    return arrived.astype(jnp.float32).sum(axis=0)


def laid_out(blocks, dim):
    blocks = jnp.moveaxis(blocks, 0, dim)
    shape = blocks.shape
    return blocks.reshape(*shape[:dim], shape[dim] * shape[dim + 1], *shape[dim + 2 :])


def turned_blocks(blocks, axes, sequence):
    shape = [lax.axis_size(a) for a in axes]
    blocks = blocks.reshape(*shape, *blocks.shape[1:])
    for k in sequence:
        blocks = lax.all_to_all(blocks, axes[k], split_axis=k, concat_axis=k, tiled=True)
    return blocks.reshape(-1, *blocks.shape[len(axes) :])


def core_and_chips(shard, groups, sequence, split_dim, concat_dim):
    peers = lax.axis_size(groups[0]) * lax.axis_size(groups[1])
    blocks = in_blocks(shard, split_dim, peers)
    return laid_out(turned_blocks(blocks, groups, sequence), concat_dim)


def from_everyone(shard, axis):
    copies = jnp.broadcast_to(shard, (lax.axis_size(axis), *shard.shape))
    return lax.all_to_all(copies, axis, split_axis=0, concat_axis=0, tiled=True)


def collect(shard, axis, dim):
    blocks = from_everyone(shard, axis)
    return laid_out(blocks, dim)


def attend_terms(query_grid, bias_grid, key_block, value_block, live, carried):
    kv_local = bias_grid.shape[0]
    key_count = key_block.shape[0]
    logits = (
        jnp.einsum(
            "qgrd,sgd->grqs",
            query_grid,
            key_block.reshape(key_count, kv_local, DH),
            preferred_element_type=jnp.float32,
        )
        * DH ** (-0.5)
        + bias_grid[:, :, None, None]
    )
    keep = jnp.where(live, jax.nn.log_sigmoid(-logits), 0.0)
    after = lax.cumsum(keep, axis=3, reverse=True) - keep + carried[:, :, :, None]
    weight = jnp.where(live, jnp.exp(jax.nn.log_sigmoid(logits) + after), 0.0).astype(jnp.bfloat16)
    partial_mix = jnp.einsum(
        "grqs,sgd->qgrd",
        weight,
        value_block.reshape(key_count, kv_local, DH),
        preferred_element_type=jnp.float32,
    )
    return (partial_mix, jnp.sum(keep, axis=3))


def local(
    queries,
    keys,
    values,
    head_bias,
    documents,
    w_out,
    resid,
    norm_gain,
    expert_ids,
    expert_gates,
    w_gate,
    w_up,
    w_down,
):
    tok_count = queries.shape[0]
    kv_local = keys.shape[1] // DH
    group_size = HEADS // KV_HEADS
    sp_count = lax.axis_size(SP)
    tp_count = lax.axis_size("tp")
    sp_index = lax.axis_index(SP)
    query_grid = queries.reshape(tok_count, kv_local, group_size, DH)
    bias_grid = head_bias.reshape(kv_local, group_size)
    doc_here = documents.astype(jnp.bfloat16)
    doc_column = doc_here.reshape(tok_count, 1)
    local_pos = jnp.arange(tok_count, dtype=jnp.int32)
    live_local = (local_pos[None, :] < local_pos[:, None]) & (
        documents[None, :] == documents[:, None]
    )
    zero_carry = jnp.zeros((kv_local, group_size, tok_count), jnp.float32)
    mix_total, carried = attend_terms(query_grid, bias_grid, keys, values, live_local, zero_carry)
    all_keys, all_values, all_docs = sent_together((keys, values, doc_column), SP, 0, 1)

    def visit(turn_index, state):
        mix_sum, carry_sum = state
        first = (sp_index - turn_index) * tok_count
        key_block = lax.dynamic_slice_in_dim(all_keys, first, tok_count, 0)
        value_block = lax.dynamic_slice_in_dim(all_values, first, tok_count, 0)
        doc_block = lax.dynamic_slice_in_dim(all_docs, first, tok_count, 0)
        live = doc_block[:, 0][None, :] == doc_here[:, None]
        partial_mix, block_keep = attend_terms(
            query_grid, bias_grid, key_block, value_block, live, carry_sum
        )
        return (mix_sum + partial_mix, carry_sum + block_keep)

    mix_total, carried = lax.fori_loop(1, sp_index + 1, visit, (mix_total, carried))
    mixed = mix_total.reshape(tok_count, kv_local * group_size * DH).astype(jnp.bfloat16)
    projected = summed_on_arrival(
        jnp.dot(mixed, w_out, preferred_element_type=jnp.float32).astype(jnp.bfloat16), "tp", 0
    )
    middle = (resid.astype(jnp.float32) + projected).astype(jnp.bfloat16)
    middle_value = middle.astype(jnp.float32)
    normed = (
        middle_value
        * lax.rsqrt(jnp.mean(middle_value * middle_value, axis=1, keepdims=True) + 1e-06)
        * norm_gain
    ).astype(jnp.bfloat16)
    row_count = normed.shape[0]
    expert_count = w_gate.shape[0] * sp_count
    slot_limit = min(row_count, max(2, 2 * TOPK * row_count // expert_count))
    flat_ids = expert_ids.reshape(-1)
    onehot_ids = (flat_ids[:, None] == jnp.arange(expert_count, dtype=jnp.int32)[None, :]).astype(
        jnp.int32
    )
    earlier = jnp.cumsum(onehot_ids, axis=0) - onehot_ids
    slot_ids = jnp.sum(earlier * onehot_ids, axis=1)
    target = flat_ids * slot_limit + slot_ids
    placing = (
        jnp.arange(expert_count * slot_limit, dtype=jnp.int32)[:, None] == target[None, :]
    ).astype(jnp.bfloat16)
    by_token = jnp.sum(placing.reshape(expert_count * slot_limit, row_count, TOPK), axis=2)
    outgoing = jnp.dot(by_token, normed, preferred_element_type=jnp.float32).astype(jnp.bfloat16)
    outgoing = outgoing.reshape(expert_count, slot_limit, D)
    arrived = core_and_chips(outgoing, ("sp_0", "sp_1"), (0, 1), 0, 0)
    gathered = collect(arrived, "tp", 0)
    expert_rows = gathered.reshape(-1, D)
    gate_value = jnp.dot(expert_rows, w_gate[0], preferred_element_type=jnp.float32)
    up_value = jnp.dot(expert_rows, w_up[0], preferred_element_type=jnp.float32)
    hidden = (jax.nn.silu(gate_value) * up_value).astype(jnp.bfloat16)
    partial_out = jnp.dot(hidden, w_down[0], preferred_element_type=jnp.float32)
    summed = summed_on_arrival(
        partial_out.reshape(tp_count, sp_count * slot_limit, D).astype(jnp.bfloat16), "tp", 0
    )
    expert_result = summed.reshape(sp_count, slot_limit, D).astype(jnp.bfloat16)
    returned = lax.all_to_all(expert_result, SP, split_axis=0, concat_axis=0, tiled=True)
    routed = jnp.dot(placing.T, returned.reshape(-1, D), preferred_element_type=jnp.float32)
    combined = jnp.sum(expert_gates[:, :, None] * routed.reshape(row_count, TOPK, D), axis=1)
    return (middle_value + combined).astype(jnp.bfloat16)


def solution(mesh):
    finer = Mesh(
        mesh.devices.reshape(mesh.shape["grp"], 16, 2, mesh.shape["tp"]),
        ("grp", "sp_0", "sp_1", "tp"),
    )
    in_specs = (
        P(GRP_SP, "tp"),
        P(GRP_SP, "tp"),
        P(GRP_SP, "tp"),
        P("tp"),
        P(GRP_SP),
        P("tp", None),
        P(GRP_SP_TP, None),
        P(),
        P(GRP_SP_TP, None),
        P(GRP_SP_TP, None),
        P(SP, None, "tp"),
        P(SP, None, "tp"),
        P(SP, "tp", None),
    )
    out_specs = P(GRP_SP_TP, None)
    return jax.shard_map(local, mesh=finer, in_specs=in_specs, out_specs=out_specs, check_vma=False)
```

profile of v0, /device:TPU:33, one launch (start us, length us, event | category | flops | bytes accessed | tf_op | source)
XLA Modules:
  0.0 632.0 jit_solution(17830155713770749261)
XLA Ops:
  6.6 0.8 fusion.63
  7.4 1.1 copy.104
  8.5 1.0 copy.105
  9.4 0.7 pad_maximum_fusion
  10.1 0.1 all-gather.2.cloned.1.call-update
  10.1 1.5 reshape.100
  11.6 1.5 reshape.102
  13.1 0.7 add.107
  13.8 0.8 copy.108
  14.6 0.1 reshape.105
  14.7 1.0 copy.99
  15.7 0.8 copy.107
  16.5 0.8 fusion.54
  17.3 1.8 fusion.60
  19.2 5.1 reduce_window_sum.27
  24.3 1.6 convolution_bitcast_fusion.1
  25.9 0.9 copy.106
  26.8 0.1 fusion.55
  26.9 0.1 reduce_window_sum.28
  26.9 77.6 %all-gather.2.cloned.1.call-done = bf16[4096,513]{0,1:T(8,128)(2,1)} async-done(((bf16[128,513]{0,1:T(8,128)(2,1)}), bf16[4096,513]{0,1:T(8,128)(2,1)}) %all-gather.2.cloned.1.call-update) | async-done | bytes 4202512 | tf_op jit(solution)/shard_map/all_gather | solution.py:20
  104.5 1.4 split.13
  106.0 4.7 fusion.62
  110.7 0.0 copy-done.8
  110.7 11.1 %while.12 = (s32[]{:T(128)}, f32[128,2,2,128]{0,3,2,1:T(8,128)}, f32[2,2,128]{2,1,0:T(2,128)S(1)}, s32[]{:T(128)}, s32[]{:T(128)}, /*index=5*/bf16[4096,256]{0,1...) while((s32[]{:T(128)}, f32[128,2,2,128]{0,3,2,1:T(8,128)}, ...), condition=%wide.region_5.6_spmd, body=%wide.region_2.5_spmd.sunk | while | flops 44056584 | bytes 2682131 | solution.py:135
  110.7 0.6 fusion.86
  111.3 0.1 add.200
  111.4 0.1 broadcast_compare_fusion.2
  111.5 0.9 constant_dynamic-slice_fusion.4
  112.4 2.0 fusion.87
  114.4 5.1 reduce_window_sum.30
  119.5 2.4 fusion.88
  121.8 1.0 convert_element_type.62
  122.8 0.0 copy-start.2
  122.8 0.0 copy-start.4
  122.8 2.9 convolution_convert_fusion.1
  125.8 4.2 all-to-all-start
  130.0 0.2 select_reduce_fusion
  130.2 0.1 reduce_sum.83
  130.3 0.1 copy.109
  130.4 0.1 fusion.58
  130.4 6.5 %all-to-all-done = bf16[4,32,2048]{2,1,0:T(8,128)(2,1)} async-done(((bf16[4,32,2048]{2,1,0:T(8,128)(2,1)}), bf16[4,32,2048]{2,1,0:T(8,128)(2,1)}, u32[]{:S(2)}, u32[]{:S(2)}) %all-to-all-start) | async-done | bytes 524320 | tf_op jit(solution)/shard_map/all_to_all | solution.py:31
  136.9 1.1 convert_reduce_fusion
  138.1 0.2 fusion.35
  138.2 1.1 convolution_convert_fusion
  139.4 2.0 reshape_reshape_reshape.3
  141.4 356.2 %all_to_all.30 = bf16[16,2,1,4,2048]{4,3,1,2,0:T(4,128)(2,1)S(1)} all-to-all(bf16[16,2,1,4,2048]{4,3,1,2,0:T(4,128)(2,1)} %bitcast.78), channel_id=1, replica_groups=mesh['grp'=2,'sp_0'=16,'sp_1'=2,'tp'=4] {'sp_0'}, dimensions={0} | all-to-all | bytes 1048576 | tf_op jit(solution)/shard_map/all_to_all | solution.py:45
  497.7 0.2 copy.111
  497.9 3.8 all_to_all.31
  501.7 0.2 copy.112
  501.9 1.0 broadcast_in_dim.21
  503.0 29.3 %all_to_all.32 = bf16[4,32,4,2048]{3,2,1,0:T(4,128)(2,1)} all-to-all(bf16[4,32,4,2048]{3,2,1,0:T(4,128)(2,1)S(1)} %broadcast_in_dim.21), channel_id=1, replica_groups=mesh['grp'=2,'sp_0'=16,'sp_1'=2,'tp'=4] {'tp'}, dimensions={0} | all-to-all | bytes 4194304 | tf_op jit(solution)/shard_map/all_to_all | solution.py:57
  532.3 4.0 reshape_reshape.7
  536.3 4.5 fusion.22
  540.7 1.9 multiply_convert_fusion
  542.7 1.8 fusion.27
  544.5 28.5 %all_to_all.33 = bf16[4,1,128,2048]{3,2,1,0:T(8,128)(2,1)} all-to-all(bf16[4,1,128,2048]{3,2,1,0:T(8,128)(2,1)S(1)} %fusion.27), channel_id=1, replica_groups=mesh['grp'=2,'sp_0'=16,'sp_1'=2,'tp'=4] {'tp'}, dimensions={0} | all-to-all | bytes 4194304 | tf_op jit(solution)/shard_map/all_to_all | solution.py:31
  573.0 2.9 reduce_sum.86
  575.9 2.1 convert_element_type.74
  577.9 9.8 %all-to-all-start.5 = ((bf16[32,4,2048]{2,1,0:T(4,128)(2,1)}), bf16[32,4,2048]{2,1,0:T(4,128)(2,1)}, u32[]{:S(2)}, u32[]{:S(2)}) async-start(bf16[32,4,2048]{2,1,0:T(4,128)(2,1)} %convert_element_type.74), calls=%async_computation.5 | async-start | bytes 1048576 | tf_op jit(solution)/shard_map/all_to_all | solution.py:174
  587.8 0.1 iota_compare_fusion.3
  587.9 33.3 %all-to-all-done.5 = bf16[32,4,2048]{2,1,0:T(4,128)(2,1)} async-done(((bf16[32,4,2048]{2,1,0:T(4,128)(2,1)}), bf16[32,4,2048]{2,1,0:T(4,128)(2,1)}, u32[]{:S(2)}, u32[]{:S(2)}) %all-to-all-start.5) | async-done | bytes 524320 | tf_op jit(solution)/shard_map/all_to_all | solution.py:174
  621.1 2.0 reshape.113
  623.1 1.3 fusion.32
  624.4 0.7 fusion.38
  (21 shorter events, 0.1 us)
Async XLA Ops:
  6.5 536.1 %copy-start = (bf16[1,768,2048]{2,1,0:T(8,128)(2,1)S(1)}, bf16[1,768,2048]{2,1,0:T(8,128)(2,1)}, u32[]{:S(2)}) copy-start(bf16[1,768,2048]{2,1,0:T(8,128)(2,1)} %param.27) | copy-start | bytes 9437188
  6.6 98.0 %all-gather.2.cloned.1.call-start = ((), (), s32[]{:S(2)}) async-start(), calls=%async_computation.6 | async-start | bytes 4392960 | tf_op jit(solution)/shard_map/all_gather | solution.py:20
  17.3 1.9 copy-start.3
  106.0 4.7 copy-start.8
  121.8 8.5 %copy-start.5 = (s32[32,2]{0,1:T(2,128)S(1)}, s32[32,2]{0,1:T(2,128)}, u32[]{:S(2)}) copy-start(s32[32,2]{0,1:T(2,128)} %param.23) | copy-start | bytes 772
  122.8 15.2 %copy-start.2 = (bf16[32,2048]{1,0:T(8,128)(2,1)S(1)}, bf16[32,2048]{1,0:T(8,128)(2,1)}, u32[]{:S(2)}) copy-start(bf16[32,2048]{1,0:T(8,128)(2,1)} %param.21) | copy-start | bytes 393220
  122.8 15.4 %copy-start.4 = (f32[2048]{0:T(1024)S(1)}, f32[2048]{0:T(1024)}, u32[]{:S(2)}) copy-start(f32[2048]{0:T(1024)} %param.22) | copy-start | bytes 24580
  125.8 11.2 %all-to-all-start = ((bf16[4,32,2048]{2,1,0:T(8,128)(2,1)}), bf16[4,32,2048]{2,1,0:T(8,128)(2,1)}, u32[]{:S(2)}, u32[]{:S(2)}) async-start(bf16[4,32,2048]{2,1,0:T(8,128)(2,1)} %bitcast.79), calls=%async_computation | async-start | bytes 1048576 | tf_op jit(solution)/shard_map/all_to_all | solution.py:31
  536.3 4.5 copy-start.1
  536.3 4.5 copy-start.7
  575.9 47.2 %copy-start.6 = (f32[32,2]{0,1:T(2,128)S(1)}, f32[32,2]{0,1:T(2,128)}, u32[]{:S(2)}) copy-start(f32[32,2]{0,1:T(2,128)} %param.24) | copy-start | bytes 772
  577.9 43.2 %all-to-all-start.5 = ((bf16[32,4,2048]{2,1,0:T(4,128)(2,1)}), bf16[32,4,2048]{2,1,0:T(4,128)(2,1)}, u32[]{:S(2)}, u32[]{:S(2)}) async-start(bf16[32,4,2048]{2,1,0:T(4,128)(2,1)} %convert_element_type.74), calls=%async_computation.5 | async-start | bytes 1048576 | tf_op jit(solution)/shard_map/all_to_all | solution.py:174
Sparse Core Ops, SparseCore 0:
  10.3 94.2 all-gather.1
where the time goes:
time: 636 us; the launch traced here: 632 us
  blocking collectives  418 us (66%)
  waiting for transfers between devices  117 us (18%)
  local copies, waits for them, and re-layouts  28.8 us (5%)
  matrix products  21.3 us (3%)
  other arithmetic  19 us (3%)
  starting transfers between devices  14 us (2%)
  between operations  13.6 us (2%)
    all_to_all x2, blocking collectives, turned_blocks(): lax.all_to_all(blocks, axes[k], split_axis=k, concat_axis=k, tiled=True)  360 us
    all_gather x1, waiting for transfers between devices, sent_together(): filled = lax.all_gather(both, axis, axis=dim, tiled=True)  77.6 us
    all_to_all x1, waiting for transfers between devices, local(): lax.all_to_all(expert_result, SP, split_axis=0, concat_axis=0, tiled=True)  33.3 us
    all_to_all x1, blocking collectives, from_everyone(): return lax.all_to_all(copies, axis, split_axis=0, concat_axis=0, tiled=True)  29.3 us
    all_to_all x1, blocking collectives, summed_on_arrival(): lax.all_to_all(blocks, axis, split_axis=0, concat_axis=0, tiled=True)  28.5 us
  transfers between devices with their start and end apart: 3, of which 3 were waited for; matrix products, arithmetic and copies ran while one was open for 3% of the time, Pallas kernels for 0%

commit v1 on v0

v1 whole, which is shorter than its diff:
```python
import functools
import math

import jax
import jax.numpy as jnp
from jax import lax
from jax.experimental import pallas as pl
from jax.experimental.pallas import tpu as pltpu
from jax.sharding import PartitionSpec as P

D = 2048
HEADS = 16
KV_HEADS = 8
DH = 128
TOPK = 2
SP = "sp"
GRP_SP = ("grp", "sp")
GRP_SP_TP = ("grp", "sp", "tp")


def sent_together(arrays, axis, dim, along):
    widths = [a.shape[along] for a in arrays]
    both = jnp.concatenate(arrays, axis=along)
    filled = lax.all_gather(both, axis, axis=dim, tiled=True)
    return tuple(jnp.split(filled, [sum(widths[:k]) for k in range(1, len(widths))], axis=along))


def in_blocks(shard, dim, peers):
    before, after = (shard.shape[:dim], shard.shape[dim + 1 :])
    return jnp.moveaxis(shard.reshape(*before, peers, -1, *after), dim, 0)


def summed_on_arrival(shard, axis, dim):
    blocks = in_blocks(shard, dim, lax.axis_size(axis))
    arrived = lax.all_to_all(blocks, axis, split_axis=0, concat_axis=0, tiled=True)
    return arrived.astype(jnp.float32).sum(axis=0)


def laid_out(blocks, dim):
    blocks = jnp.moveaxis(blocks, 0, dim)
    shape = blocks.shape
    return blocks.reshape(*shape[:dim], shape[dim] * shape[dim + 1], *shape[dim + 2 :])


def turned_blocks(blocks, axes, sequence):
    shape = [lax.axis_size(a) for a in axes]
    blocks = blocks.reshape(*shape, *blocks.shape[1:])
    for k in sequence:
        blocks = lax.all_to_all(blocks, axes[k], split_axis=k, concat_axis=k, tiled=True)
    return blocks.reshape(-1, *blocks.shape[len(axes) :])


def core_and_chips(shard, groups, sequence, split_dim, concat_dim):
    peers = lax.axis_size(groups[0]) * lax.axis_size(groups[1])
    blocks = in_blocks(shard, split_dim, peers)
    return laid_out(turned_blocks(blocks, groups, sequence), concat_dim)


def from_everyone(shard, axis):
    copies = jnp.broadcast_to(shard, (lax.axis_size(axis), *shard.shape))
    return lax.all_to_all(copies, axis, split_axis=0, concat_axis=0, tiled=True)


def collect(shard, axis, dim):
    blocks = from_everyone(shard, axis)
    return laid_out(blocks, dim)


MESH_ID = pl.DeviceIdType.MESH
LOG2E = math.log2(math.e)


def remote(src, dst, send, recv, axis, index):
    return pltpu.make_async_remote_copy(
        src_ref=src,
        dst_ref=dst,
        send_sem=send,
        recv_sem=recv,
        device_id={axis: index},
        device_id_type=MESH_ID,
    )


def attention_kernel(
    chips,
    reach,
    q_ref,
    k_ref,
    v_ref,
    doc_row_ref,
    doc_col_ref,
    bias_ref,
    out_ref,
    kv,
    qx,
    doc_col,
    tri,
    near,
    far,
    carry,
    mix,
    mixed_in,
    pair_send,
    pair_recv,
    own_sem,
    up_send,
    up_recv,
    down_send,
    down_recv,
    back_send,
    back_recv,
):
    tok = q_ref.shape[0]
    both = 2 * tok
    me = lax.axis_index("sp")
    chip = me // 2
    core = me % 2
    other = 1 - core
    partner = chip * 2 + other
    up = lax.rem(chip + 1, chips) * 2 + core
    down = lax.rem(chip + chips - 1, chips) * 2 + core
    up_steps = chips // 2
    down_steps = chips - 1 - up_steps

    barrier = pltpu.get_barrier_semaphore()
    for peer in (partner, up, down):
        pl.semaphore_signal(barrier, inc=1, device_id={"sp": peer}, device_id_type=MESH_ID)

    def at(x, size=None):
        return pl.ds(pl.multiple_of(x, 128), size or tok)

    doc_rows = doc_row_ref.shape[0]
    rows_here = at(core * tok)
    moves = []
    for h in range(2):
        moves.append((lambda o, h=h: q_ref.at[:, at(o * 256 + h * 128, 128)], qx.at[at(h * both + core * tok), :]))
    moves.append((lambda o: k_ref.at[:, at(o * 128, 128)], kv.at[chip, rows_here, :]))
    moves.append((lambda o: v_ref.at[:, at(o * 128, 128)], kv.at[chip, at(both + core * tok), :]))
    moves.append(
        (
            lambda o: doc_row_ref,
            kv.at[chip, pl.ds(pl.multiple_of(2 * both + core * doc_rows, doc_rows), doc_rows), :],
        )
    )
    moves.append((lambda o: doc_col_ref, doc_col.at[rows_here, :]))
    kept = [pltpu.make_async_copy(src(core), dst, own_sem.at[i]) for i, (src, dst) in enumerate(moves)]
    for copy in kept:
        copy.start()
    pl.semaphore_wait(barrier, 3)
    traded = [
        remote(src(other), dst, pair_send.at[i], pair_recv.at[i], "sp", partner)
        for i, (src, dst) in enumerate(moves)
    ]
    for i in (2, 3, 4, 0, 1, 5):
        traded[i].start()
    row_id = lax.broadcasted_iota(jnp.int32, (both, both), 0)
    col_id = lax.broadcasted_iota(jnp.int32, (both, both), 1)
    tri[...] = (row_id > col_id).astype(jnp.bfloat16)
    near[...] = jnp.zeros_like(near)
    far[...] = jnp.zeros_like(far)
    carry[...] = jnp.zeros_like(carry)

    pieces = ((0, both), (both, both + 2 * doc_rows))

    def upward(step, piece):
        block = lax.rem(chip - step + chips, chips)
        first, count = pieces[piece]
        ref = kv.at[block, pl.ds(first, count), :]
        return remote(ref, ref, up_send.at[step, piece], up_recv.at[step, piece], "sp", up)

    def downward(step, piece):
        block = lax.rem(chip + step, chips)
        first, count = pieces[piece]
        ref = kv.at[block, pl.ds(first, count), :]
        return remote(ref, ref, down_send.at[step, piece], down_recv.at[step, piece], "sp", down)

    def arrived_up(step, piece):
        block = lax.rem(chip - step - 1 + chips, chips)
        first, count = pieces[piece]
        ref = kv.at[block, pl.ds(first, count), :]
        return remote(ref, ref, up_send.at[step, piece], up_recv.at[step, piece], "sp", up)

    def arrived_down(step, piece):
        block = lax.rem(chip + step + 1, chips)
        first, count = pieces[piece]
        ref = kv.at[block, pl.ds(first, count), :]
        return remote(ref, ref, down_send.at[step, piece], down_recv.at[step, piece], "sp", down)

    for i in (2, 3, 4):
        kept[i].wait()
    traded[2].wait_recv()
    upward(0, 0).start()
    downward(0, 0).start()
    traded[3].wait_recv()
    traded[4].wait_recv()
    upward(0, 1).start()
    downward(0, 1).start()
    for i in (0, 1, 5):
        kept[i].wait()
        traded[i].wait_recv()

    scale = LOG2E / math.sqrt(128.0)

    def piece_of(block, i, diagonal):
        rows = pl.ds(i * tok, tok)
        head, first = i // 2, (i % 2) * tok
        logits = lax.dot_general(
            qx[rows, :],
            kv[block, 0:both, :],
            (((1,), (1,)), ((), ())),
            preferred_element_type=jnp.float32,
        )
        logits = logits * scale + bias_ref[2 * core + head] * LOG2E
        tail = jnp.log(1.0 + jnp.exp2(-jnp.abs(logits))) * LOG2E
        spend = jnp.maximum(logits, 0.0) + tail
        gain = jnp.minimum(logits, 0.0) - tail
        doc_here = doc_col[pl.ds(first, tok), :].astype(jnp.float32)
        doc_here = jnp.concatenate([doc_here, doc_here], axis=1)
        low = kv[block, 2 * both : 2 * both + doc_rows, :].astype(jnp.float32)
        high = kv[block, 2 * both + doc_rows : 2 * both + 2 * doc_rows, :].astype(jnp.float32)
        doc_there = jnp.concatenate([low[0:1], high[0:1]], axis=1)
        live = doc_here == doc_there
        if diagonal:
            t = first + lax.broadcasted_iota(jnp.int32, (tok, both), 0)
            s = lax.broadcasted_iota(jnp.int32, (tok, both), 1)
            live = live & (s < t)
            spend = jnp.where(live, spend, 0.0)
        coarse = spend.astype(jnp.bfloat16)
        fine = (spend - coarse.astype(jnp.float32)).astype(jnp.bfloat16)
        later = jnp.dot(coarse, tri[...], preferred_element_type=jnp.float32) + jnp.dot(
            fine, tri[...], preferred_element_type=jnp.float32
        )
        weight = jnp.where(live, jnp.exp2(gain - later), 0.0).astype(jnp.bfloat16)
        share = jnp.dot(weight, kv[block, both : 2 * both, :], preferred_element_type=jnp.float32)
        whole = jnp.broadcast_to(later[:, 0:1] + spend[:, 0:1], (tok, 128))
        return rows, share, whole

    for i in range(4):
        rows, share, whole = piece_of(chip, i, True)
        near[rows, :] = share
        carry[rows, :] = whole

    def visit(step, _):
        for piece in range(2):
            arrived_up(step, piece).wait_recv()

            @pl.when(step + 1 < up_steps)
            def _():
                upward(step + 1, piece).start()

            @pl.when(step < down_steps)
            def _():
                arrived_down(step, piece).wait_recv()

                @pl.when(step + 1 < down_steps)
                def _():
                    downward(step + 1, piece).start()

        @pl.when(chip - step - 1 >= 0)
        def _():
            for i in range(4):
                rows, share, whole = piece_of(chip - step - 1, i, False)
                near[rows, :] += jnp.exp2(-carry[rows, :]) * share
                carry[rows, :] += whole

        wrapped = chip + step + 1 - chips

        @pl.when((step < down_steps) & (wrapped >= 0) & (chip - wrapped <= reach))
        def _():
            for i in range(4):
                rows, share, whole = piece_of(wrapped, i, False)
                far[rows, :] = jnp.exp2(-whole) * far[rows, :] + share

        return 0

    lax.fori_loop(0, up_steps, visit, 0)

    for h in range(2):
        rows = pl.ds(h * both, both)
        mix[h] = (near[rows, :] + jnp.exp2(-carry[rows, :]) * far[rows, :]).astype(jnp.bfloat16)
    back = [
        remote(
            mix.at[h, at(other * tok), :],
            mixed_in.at[h],
            back_send.at[h],
            back_recv.at[h],
            "sp",
            partner,
        )
        for h in range(2)
    ]
    for copy in back:
        copy.start()
    for h in range(2):
        out_ref[:, at(core * 256 + h * 128, 128)] = mix[h, at(core * tok), :]
    for h in range(2):
        back[h].wait_recv()
        out_ref[:, at(other * 256 + h * 128, 128)] = mixed_in[h]
    for copy in traded + back:
        copy.wait_send()

    def drain(step, _):
        for piece in range(2):
            upward(step, piece).wait_send()

            @pl.when(step < down_steps)
            def _():
                downward(step, piece).wait_send()

        return 0

    lax.fori_loop(0, up_steps, drain, 0)


def attention(queries, keys, values, head_bias, documents, chips):
    tok = queries.shape[0]
    both = 2 * tok
    doc = documents.astype(jnp.bfloat16)
    doc_rows = 16
    doc_row = jnp.broadcast_to(doc[None, :], (doc_rows, tok))
    doc_col = jnp.broadcast_to(doc[:, None], (tok, 128))
    longest = chips * both * 3 // 4
    reach = (longest - 1 + both - 1) // both
    up_steps = chips // 2
    vmem = pl.BlockSpec(memory_space=pltpu.VMEM)
    dma = pltpu.SemaphoreType.DMA
    return pl.pallas_call(
        functools.partial(attention_kernel, chips, reach),
        out_shape=jax.ShapeDtypeStruct((tok, 512), jnp.bfloat16),
        in_specs=[vmem] * 5 + [pl.BlockSpec(memory_space=pltpu.SMEM)],
        out_specs=vmem,
        scratch_shapes=[
            pltpu.VMEM((chips, 2 * both + 2 * doc_rows, 128), jnp.bfloat16),
            pltpu.VMEM((2 * both, 128), jnp.bfloat16),
            pltpu.VMEM((both, 128), jnp.bfloat16),
            pltpu.VMEM((both, both), jnp.bfloat16),
            pltpu.VMEM((2 * both, 128), jnp.float32),
            pltpu.VMEM((2 * both, 128), jnp.float32),
            pltpu.VMEM((2 * both, 128), jnp.float32),
            pltpu.VMEM((2, both, 128), jnp.bfloat16),
            pltpu.VMEM((2, tok, 128), jnp.bfloat16),
            dma((6,)),
            dma((6,)),
            dma((6,)),
            dma((up_steps, 2)),
            dma((up_steps, 2)),
            dma((up_steps, 2)),
            dma((up_steps, 2)),
            dma((2,)),
            dma((2,)),
        ],
        compiler_params=pltpu.CompilerParams(collective_id=0, has_side_effects=True),
        name="attention",
    )(queries, keys, values, doc_row, doc_col, head_bias)


def local(
    queries,
    keys,
    values,
    head_bias,
    documents,
    w_out,
    resid,
    norm_gain,
    expert_ids,
    expert_gates,
    w_gate,
    w_up,
    w_down,
):
    sp_count = lax.axis_size("sp")
    tp_count = lax.axis_size("tp")
    mixed = attention(queries, keys, values, head_bias, documents, sp_count // 2)
    projected = summed_on_arrival(
        jnp.dot(mixed, w_out, preferred_element_type=jnp.float32).astype(jnp.bfloat16), "tp", 0
    )
    middle = (resid.astype(jnp.float32) + projected).astype(jnp.bfloat16)
    middle_value = middle.astype(jnp.float32)
    normed = (
        middle_value
        * lax.rsqrt(jnp.mean(middle_value * middle_value, axis=1, keepdims=True) + 1e-06)
        * norm_gain
    ).astype(jnp.bfloat16)
    row_count = normed.shape[0]
    expert_count = w_gate.shape[0] * sp_count
    slot_limit = min(row_count, max(2, 2 * TOPK * row_count // expert_count))
    flat_ids = expert_ids.reshape(-1)
    onehot_ids = (flat_ids[:, None] == jnp.arange(expert_count, dtype=jnp.int32)[None, :]).astype(
        jnp.int32
    )
    earlier = jnp.cumsum(onehot_ids, axis=0) - onehot_ids
    slot_ids = jnp.sum(earlier * onehot_ids, axis=1)
    target = flat_ids * slot_limit + slot_ids
    placing = (
        jnp.arange(expert_count * slot_limit, dtype=jnp.int32)[:, None] == target[None, :]
    ).astype(jnp.bfloat16)
    by_token = jnp.sum(placing.reshape(expert_count * slot_limit, row_count, TOPK), axis=2)
    outgoing = jnp.dot(by_token, normed, preferred_element_type=jnp.float32).astype(jnp.bfloat16)
    outgoing = outgoing.reshape(expert_count, slot_limit, D)
    arrived = lax.all_to_all(outgoing, "sp", split_axis=0, concat_axis=0, tiled=True)
    gathered = collect(arrived, "tp", 0)
    expert_rows = gathered.reshape(-1, D)
    gate_value = jnp.dot(expert_rows, w_gate[0], preferred_element_type=jnp.float32)
    up_value = jnp.dot(expert_rows, w_up[0], preferred_element_type=jnp.float32)
    hidden = (jax.nn.silu(gate_value) * up_value).astype(jnp.bfloat16)
    partial_out = jnp.dot(hidden, w_down[0], preferred_element_type=jnp.float32)
    summed = summed_on_arrival(
        partial_out.reshape(tp_count, sp_count * slot_limit, D).astype(jnp.bfloat16), "tp", 0
    )
    expert_result = summed.reshape(sp_count, slot_limit, D).astype(jnp.bfloat16)
    returned = lax.all_to_all(expert_result, "sp", split_axis=0, concat_axis=0, tiled=True)
    routed = jnp.dot(placing.T, returned.reshape(-1, D), preferred_element_type=jnp.float32)
    combined = jnp.sum(expert_gates[:, :, None] * routed.reshape(row_count, TOPK, D), axis=1)
    return (middle_value + combined).astype(jnp.bfloat16)


def solution(mesh):
    in_specs = (
        P(GRP_SP, "tp"),
        P(GRP_SP, "tp"),
        P(GRP_SP, "tp"),
        P("tp"),
        P(GRP_SP),
        P("tp", None),
        P(GRP_SP_TP, None),
        P(),
        P(GRP_SP_TP, None),
        P(GRP_SP_TP, None),
        P(SP, None, "tp"),
        P(SP, None, "tp"),
        P(SP, "tp", None),
    )
    out_specs = P(GRP_SP_TP, None)
    return jax.shard_map(local, mesh=mesh, in_specs=in_specs, out_specs=out_specs, check_vma=False)
```

time: 636 us -> 247 us (0.39)
  blocking collectives: 418 us -> 99.3 us
  waiting for transfers between devices: 117 us -> 41.8 us
  Pallas kernels: 0 us -> 60.7 us
  local copies, waits for them, and re-layouts: 28.8 us -> 12.8 us
  between operations: 13.6 us -> 0.16 us
  other arithmetic: 19 us -> 6.24 us
  matrix products: 21.3 us -> 13.5 us
    all_to_all x2 -> x1, blocking collectives: 360 us -> 42.1 us  [local(): lax.all_to_all(outgoing, 'sp', split_axis=0, concat_axis=0, tiled=True)]
    all_gather x1 -> x0, waiting for transfers between devices: 77.6 us -> none  [sent_together(): filled = lax.all_gather(both, axis, axis=dim, tiled=True)]
    pallas_call x0 -> x1, Pallas kernels: none -> 60.7 us  [attention(): pl.pallas_call(functools.partial(attention_kernel, chips, reach), out_sha...]
    another operation x2 -> x0, other arithmetic: 10.2 us -> none  [attend_terms(): lax.cumsum(keep, axis=3, reverse=True) - keep + carried[:, :, :, None]]
    dot_general x4 -> x0, matrix products: 7.77 us -> none  [the longest x2 3.94 us: attend_terms(): jnp.einsum('grqs,sgd->qgrd', weight, value_block.reshape(key_count, kv_lo...]
  transfers between devices with their start and end apart: 3 -> 2, of which waited for: 3 -> 2; matrix products, arithmetic and copies ran while one was open for 3% -> 0% of each run, Pallas kernels for 0% -> 0%
where the time goes in v1:
time: 247 us; the launch traced here: 246 us
  blocking collectives  99.3 us (40%)
  Pallas kernels  60.7 us (25%)
  waiting for transfers between devices  41.8 us (17%)
  matrix products  13.5 us (5%)
  local copies, waits for them, and re-layouts  12.8 us (5%)
  starting transfers between devices  11.2 us (5%)
  other arithmetic  6.24 us (3%)
    pallas_call x1, Pallas kernels, attention(): pl.pallas_call(functools.partial(attention_kernel, chips, reach), out_sha...  60.7 us
    all_to_all x1, blocking collectives, local(): lax.all_to_all(outgoing, 'sp', split_axis=0, concat_axis=0, tiled=True)  42.1 us
    all_to_all x1, waiting for transfers between devices, local(): lax.all_to_all(expert_result, 'sp', split_axis=0, concat_axis=0, tiled=True)  33.4 us
    all_to_all x1, blocking collectives, from_everyone(): return lax.all_to_all(copies, axis, split_axis=0, concat_axis=0, tiled=True)  29.2 us
    all_to_all x1, blocking collectives, summed_on_arrival(): lax.all_to_all(blocks, axis, split_axis=0, concat_axis=0, tiled=True)  28 us
    all_to_all x1, waiting for transfers between devices, summed_on_arrival(): lax.all_to_all(blocks, axis, split_axis=0, concat_axis=0, tiled=True)  8.44 us
    all_to_all x1, starting transfers between devices, local(): lax.all_to_all(expert_result, 'sp', split_axis=0, concat_axis=0, tiled=True)  6.89 us
  transfers between devices with their start and end apart: 2, of which 2 were waited for; matrix products, arithmetic and copies ran while one was open for 0% of the time, Pallas kernels for 0%

profile of v1, /device:TPU:33, one launch (start us, length us, event | category | flops | bytes accessed | tf_op | source)
XLA Modules:
  0.0 245.9 jit_solution(11316780076592310569)
XLA Ops:
  0.0 0.0 copy-start
  0.0 0.8 convert_element_type.48
  0.8 0.7 broadcast_in_dim.7.doc_col_ref
  1.5 0.6 broadcast_in_dim.6.doc_row_ref
  2.1 0.0 copy-start.4
  2.1 60.7 %attention.1 = bf16[128,512]{1,0:T(8,128)(2,1)} custom-call(bf16[128,512]{1,0:T(8,128)(2,1)} %q_ref.1, bf16[128,256]{1,0:T(8,128)(2,1)} %k_ref.1, bf16[128,256]{1,0:T(8,128)(2,1)} %v_ref.1, bf16[16,128]{1,0:T(8,128)(2,1)} %broadcast_in_dim.6.doc_row_ref, bf16[128,128]{1,0:T(8,128)(2,1)} %broadcast_in_dim.7.doc_col_ref, f32[4]{0:T(128)} %bias_ref.1), custom_call_target="tpu_custom_call" | custom-call | tf_op jit(solution)/shard_map/attention/pallas_call | solution.py:327
  62.9 0.0 copy-start.2
  62.9 0.0 copy-start.3
  62.9 2.9 %convolution_convert_fusion.1 = bf16[128,2048]{1,0:T(8,128)(2,1)} fusion(bf16[128,512]{1,0:T(8,128)(2,1)} %attention.1, bf16[512,2048]{1,0:T(8,128)(2,1)} %param.18), kind=kOutput, calls=%fused_computation.9 | convolution fusion | flops 268697600 | bytes 2752512 | tf_op jit(solution)/shard_map/dot_general | solution.py:376
  65.8 4.3 %all-to-all-start = ((bf16[4,32,2048]{2,1,0:T(8,128)(2,1)}), bf16[4,32,2048]{2,1,0:T(8,128)(2,1)}, u32[]{:S(2)}, u32[]{:S(2)}) async-start(bf16[4,32,2048]{2,1,0:T(8,128)(2,1)} %bitcast.29), calls=%async_computation | async-start | bytes 1048576 | tf_op jit(solution)/shard_map/all_to_all | solution.py:35
  70.1 0.0 copy-done.4
  70.1 0.1 copy.32
  70.2 0.1 reshape.79
  70.3 0.1 fusion.22
  70.4 0.1 reduce_window_sum.11
  70.5 0.2 select_reduce_fusion
  70.7 0.1 reduce_sum.64
  70.8 0.1 copy.33
  70.9 0.1 fusion.25
  71.0 8.4 %all-to-all-done = bf16[4,32,2048]{2,1,0:T(8,128)(2,1)} async-done(((bf16[4,32,2048]{2,1,0:T(8,128)(2,1)}), bf16[4,32,2048]{2,1,0:T(8,128)(2,1)}, u32[]{:S(2)}, u32[]{:S(2)}) %all-to-all-start) | async-done | bytes 524320 | tf_op jit(solution)/shard_map/all_to_all | solution.py:35
  79.4 1.1 convert_reduce_fusion
  80.6 0.0 copy-done.2
  80.6 0.2 fusion.15
  80.7 0.0 copy-done.3
  80.7 1.1 convolution_convert_fusion
  81.9 2.0 reshape.80
  83.9 42.1 %all_to_all.25 = bf16[32,4,2048]{2,1,0:T(4,128)(2,1)S(1)} all-to-all(bf16[32,4,2048]{2,1,0:T(4,128)(2,1)} %reshape.80), channel_id=1, replica_groups=mesh['grp'=2,'sp'=32,'tp'=4] {'sp'}, dimensions={0} | all-to-all | bytes 1048576 | tf_op jit(solution)/shard_map/all_to_all | solution.py:401
  126.0 1.0 broadcast_in_dim.8
  127.1 29.2 %all_to_all.26 = bf16[4,32,4,2048]{3,2,1,0:T(4,128)(2,1)} all-to-all(bf16[4,32,4,2048]{3,2,1,0:T(4,128)(2,1)S(1)} %broadcast_in_dim.8), channel_id=1, replica_groups=mesh['grp'=2,'sp'=32,'tp'=4] {'tp'}, dimensions={0} | all-to-all | bytes 4194304 | tf_op jit(solution)/shard_map/all_to_all | solution.py:61
  156.3 4.0 %reshape_reshape.3 = bf16[512,2048]{1,0:T(8,128)(2,1)} reshape(bf16[4,32,4,2048]{3,2,1,0:T(4,128)(2,1)} %all_to_all.26) | data formatting | bytes 4194304 | tf_op jit(solution)/shard_map/reshape;reshape | solution.py:403
  160.2 0.0 copy-start.1
  160.2 0.0 copy-start.6
  160.2 4.5 %fusion.4 = f32[512,768]{1,0:T(8,128)S(1)} fusion(bf16[512,2048]{1,0:T(8,128)(2,1)} %reshape_reshape.3, bf16[1,2048,768]{2,1,0:T(8,128)(2,1)} %param.23), kind=kOutput, calls=%fused_computation.4 | convolution fusion | flops 1610612736 | bytes 6815744 | tf_op jit(solution)/shard_map/dot_general | solution.py:404
  164.7 0.0 copy-done.1
  164.7 0.0 copy-done.6
  164.7 1.9 multiply_convert_fusion
  166.6 0.0 copy-done
  166.6 1.8 fusion.9
  168.5 28.0 %all_to_all.27 = bf16[4,1,128,2048]{3,2,1,0:T(8,128)(2,1)} all-to-all(bf16[4,1,128,2048]{3,2,1,0:T(8,128)(2,1)S(1)} %fusion.9), channel_id=1, replica_groups=mesh['grp'=2,'sp'=32,'tp'=4] {'tp'}, dimensions={0} | all-to-all | bytes 4194304 | tf_op jit(solution)/shard_map/all_to_all | solution.py:35
  196.5 2.9 %reduce_sum.67 = bf16[128,2048]{1,0:T(8,128)(2,1)} reduce(bf16[4,1,128,2048]{3,2,1,0:T(8,128)(2,1)} %all_to_all.27, bf16[]{:T(256)} %constant.17.clone.1), dimensions={0,1}, to_apply=%region_5.6 | reduce | flops 786432 | bytes 2621442 | tf_op jit(solution)/shard_map/reduce_sum | solution.py:36
  199.4 0.0 copy-start.5
  199.4 2.1 convert_element_type.59
  201.5 6.9 %all-to-all-start.4 = ((bf16[32,4,2048]{2,1,0:T(4,128)(2,1)}), bf16[32,4,2048]{2,1,0:T(4,128)(2,1)}, u32[]{:S(2)}, u32[]{:S(2)}) async-start(bf16[32,4,2048]{2,1,0:T(4,128)(2,1)} %convert_element_type.59), calls=%async_computation.4 | async-start | bytes 1048576 | tf_op jit(solution)/shard_map/all_to_all | solution.py:412
  208.4 0.1 iota_compare_fusion.2
  208.5 33.4 %all-to-all-done.4 = bf16[32,4,2048]{2,1,0:T(4,128)(2,1)} async-done(((bf16[32,4,2048]{2,1,0:T(4,128)(2,1)}), bf16[32,4,2048]{2,1,0:T(4,128)(2,1)}, u32[]{:S(2)}, u32[]{:S(2)}) %all-to-all-start.4) | async-done | bytes 524320 | tf_op jit(solution)/shard_map/all_to_all | solution.py:412
  241.9 2.0 reshape.84
  243.9 0.0 copy-done.5
  243.9 1.3 fusion.14
  245.2 0.7 fusion.18
  (4 shorter events, 0.0 us)
Async XLA Ops:
  0.0 166.6 %copy-start = (bf16[1,768,2048]{2,1,0:T(8,128)(2,1)S(1)}, bf16[1,768,2048]{2,1,0:T(8,128)(2,1)}, u32[]{:S(2)}) copy-start(bf16[1,768,2048]{2,1,0:T(8,128)(2,1)} %param.25) | copy-start | bytes 9437188
  2.1 68.0 %copy-start.4 = (s32[32,2]{0,1:T(2,128)S(1)}, s32[32,2]{0,1:T(2,128)}, u32[]{:S(2)}) copy-start(s32[32,2]{0,1:T(2,128)} %param.21) | copy-start | bytes 772
  62.9 17.7 %copy-start.2 = (bf16[32,2048]{1,0:T(8,128)(2,1)S(1)}, bf16[32,2048]{1,0:T(8,128)(2,1)}, u32[]{:S(2)}) copy-start(bf16[32,2048]{1,0:T(8,128)(2,1)} %param.19) | copy-start | bytes 393220
  62.9 17.9 %copy-start.3 = (f32[2048]{0:T(1024)S(1)}, f32[2048]{0:T(1024)}, u32[]{:S(2)}) copy-start(f32[2048]{0:T(1024)} %param.20) | copy-start | bytes 24580
  65.8 13.6 %all-to-all-start = ((bf16[4,32,2048]{2,1,0:T(8,128)(2,1)}), bf16[4,32,2048]{2,1,0:T(8,128)(2,1)}, u32[]{:S(2)}, u32[]{:S(2)}) async-start(bf16[4,32,2048]{2,1,0:T(8,128)(2,1)} %bitcast.29), calls=%async_computation | async-start | bytes 1048576 | tf_op jit(solution)/shard_map/all_to_all | solution.py:35
  160.2 4.5 %copy-start.1 = (bf16[512,2048]{1,0:T(8,128)(2,1)S(1)}, bf16[512,2048]{1,0:T(8,128)(2,1)}, u32[]{:S(2)}) copy-start(bf16[512,2048]{1,0:T(8,128)(2,1)} %reshape_reshape.3) | copy-start | bytes 6291460
  160.2 4.5 %copy-start.6 = (bf16[1,2048,768]{2,1,0:T(8,128)(2,1)S(1)}, bf16[1,2048,768]{2,1,0:T(8,128)(2,1)}, u32[]{:S(2)}) copy-start(bf16[1,2048,768]{2,1,0:T(8,128)(2,1)} %param.24) | copy-start | bytes 9437188
  199.4 44.4 %copy-start.5 = (f32[32,2]{0,1:T(2,128)S(1)}, f32[32,2]{0,1:T(2,128)}, u32[]{:S(2)}) copy-start(f32[32,2]{0,1:T(2,128)} %param.22) | copy-start | bytes 772
  201.5 40.4 %all-to-all-start.4 = ((bf16[32,4,2048]{2,1,0:T(4,128)(2,1)}), bf16[32,4,2048]{2,1,0:T(4,128)(2,1)}, u32[]{:S(2)}, u32[]{:S(2)}) async-start(bf16[32,4,2048]{2,1,0:T(4,128)(2,1)} %convert_element_type.59), calls=%async_computation.4 | async-start | bytes 1048576 | tf_op jit(solution)/shard_map/all_to_all | solution.py:412

commit v2 on v1

--- a/solution.py
+++ b/solution.py
@@ -8,62 +8,10 @@
 from jax.experimental.pallas import tpu as pltpu
 from jax.sharding import PartitionSpec as P
 
-D = 2048
-HEADS = 16
-KV_HEADS = 8
-DH = 128
 TOPK = 2
 SP = "sp"
 GRP_SP = ("grp", "sp")
 GRP_SP_TP = ("grp", "sp", "tp")
-
-
-def sent_together(arrays, axis, dim, along):
-    widths = [a.shape[along] for a in arrays]
-    both = jnp.concatenate(arrays, axis=along)
-    filled = lax.all_gather(both, axis, axis=dim, tiled=True)
-    return tuple(jnp.split(filled, [sum(widths[:k]) for k in range(1, len(widths))], axis=along))
-
-
-def in_blocks(shard, dim, peers):
-    before, after = (shard.shape[:dim], shard.shape[dim + 1 :])
-    return jnp.moveaxis(shard.reshape(*before, peers, -1, *after), dim, 0)
-
-
-def summed_on_arrival(shard, axis, dim):
-    blocks = in_blocks(shard, dim, lax.axis_size(axis))
-    arrived = lax.all_to_all(blocks, axis, split_axis=0, concat_axis=0, tiled=True)
-    return arrived.astype(jnp.float32).sum(axis=0)
-
-
-def laid_out(blocks, dim):
-    blocks = jnp.moveaxis(blocks, 0, dim)
-    shape = blocks.shape
-    return blocks.reshape(*shape[:dim], shape[dim] * shape[dim + 1], *shape[dim + 2 :])
-
-
-def turned_blocks(blocks, axes, sequence):
-    shape = [lax.axis_size(a) for a in axes]
-    blocks = blocks.reshape(*shape, *blocks.shape[1:])
-    for k in sequence:
-        blocks = lax.all_to_all(blocks, axes[k], split_axis=k, concat_axis=k, tiled=True)
-    return blocks.reshape(-1, *blocks.shape[len(axes) :])
-
-
-def core_and_chips(shard, groups, sequence, split_dim, concat_dim):
-    peers = lax.axis_size(groups[0]) * lax.axis_size(groups[1])
-    blocks = in_blocks(shard, split_dim, peers)
-    return laid_out(turned_blocks(blocks, groups, sequence), concat_dim)
-
-
-def from_everyone(shard, axis):
-    copies = jnp.broadcast_to(shard, (lax.axis_size(axis), *shard.shape))
-    return lax.all_to_all(copies, axis, split_axis=0, concat_axis=0, tiled=True)
-
-
-def collect(shard, axis, dim):
-    blocks = from_everyone(shard, axis)
-    return laid_out(blocks, dim)
 
 
 MESH_ID = pl.DeviceIdType.MESH
@@ -354,6 +302,440 @@
     )(queries, keys, values, doc_row, doc_col, head_bias)
 
 
+def feed_kernel(
+    chips,
+    mixed_ref,
+    w_out_ref,
+    resid_ref,
+    gain_ref,
+    slot_row_ref,
+    slot_col_ref,
+    gate_col_ref,
+    w_gate_hbm,
+    w_up_hbm,
+    w_down_hbm,
+    out_ref,
+    w_gate,
+    w_up,
+    w_down,
+    partial,
+    first_a,
+    first_b,
+    summed,
+    second_a,
+    second_b,
+    middle,
+    stack,
+    outgoing,
+    inbox,
+    rows_in,
+    reply,
+    returned,
+    order,
+    spread,
+    weigh,
+    weight_sem,
+    self_sem,
+    z_send,
+    z_recv,
+    a_send,
+    a_recv,
+    b_send,
+    b_recv,
+    relay_send,
+    relay_recv,
+    first_send,
+    first_recv,
+    second_send,
+    second_recv,
+    reply_send,
+    reply_recv,
+):
+    waves = chips // 4
+    half_ring = chips // 2
+    peers = 2 * chips
+    rows, width = resid_ref.shape
+    quarter = width // 4
+    half = width // 2
+    me = lax.axis_index("sp")
+    tp = lax.axis_index("tp")
+    chip = me // 2
+    core = me % 2
+    low = tp % 2
+    peer_a = tp + 1 - 2 * low
+    peer_b = 3 - tp
+    across = lax.rem(tp + 2, 4)
+
+    loads = [
+        pltpu.make_async_copy(src.at[0], dst, weight_sem.at[i])
+        for i, (src, dst) in enumerate(((w_gate_hbm, w_gate), (w_up_hbm, w_up), (w_down_hbm, w_down)))
+    ]
+    for copy in loads:
+        copy.start()
+
+    barrier = pltpu.get_barrier_semaphore()
+
+    def greet(k, _):
+        pl.semaphore_signal(
+            barrier, inc=1, device_id={"sp": lax.rem(me + k, peers)}, device_id_type=MESH_ID
+        )
+        return 0
+
+    lax.fori_loop(1, peers, greet, 0)
+    for peer in (peer_a, peer_b):
+        pl.semaphore_signal(barrier, inc=1, device_id={"tp": peer}, device_id_type=MESH_ID)
+
+    def block(n, which, first=0, size=None):
+        return partial.at[n, pl.ds(pl.multiple_of(which * rows, rows), rows), pl.ds(first, size or width)]
+
+    def first_send_of(n, i):
+        owner = (peer_a, peer_b, across, across)[i]
+        into = (first_a, first_b)[i % 2].at[n, i // 2]
+        return remote(
+            block(n, owner, (i % 2) * half, half),
+            into,
+            first_send.at[n, i],
+            first_recv.at[n, i],
+            "tp",
+            (peer_a, peer_b)[i % 2],
+        )
+
+    def second_send_of(n, i):
+        into = (second_b, second_a)[i].at[n]
+        return remote(
+            summed.at[n, i], into, second_send.at[n, i], second_recv.at[n, i], "tp", (peer_b, peer_a)[i]
+        )
+
+    def sum_start(n):
+        for i in (2, 3, 0, 1):
+            first_send_of(n, i).start()
+
+    def sum_middle(n):
+        first_send_of(n, 2).wait_recv()
+        summed[n, 0] = (
+            block(n, peer_b, 0, half)[...].astype(jnp.float32) + first_a[n, 1].astype(jnp.float32)
+        ).astype(jnp.bfloat16)
+        second_send_of(n, 0).start()
+        first_send_of(n, 3).wait_recv()
+        summed[n, 1] = (
+            block(n, peer_a, half, half)[...].astype(jnp.float32) + first_b[n, 1].astype(jnp.float32)
+        ).astype(jnp.bfloat16)
+        second_send_of(n, 1).start()
+
+    def sum_end(n):
+        first_send_of(n, 0).wait_recv()
+        first_send_of(n, 1).wait_recv()
+        left = block(n, tp, 0, half)[...].astype(jnp.float32) + first_a[n, 0].astype(jnp.float32)
+        right = block(n, tp, half, half)[...].astype(jnp.float32) + first_b[n, 0].astype(jnp.float32)
+        second_send_of(n, 0).wait_recv()
+        left = left + second_b[n].astype(jnp.float32)
+        second_send_of(n, 1).wait_recv()
+        right = right + second_a[n].astype(jnp.float32)
+        return left, right
+
+    for j in range(4):
+        columns = pl.ds(j * quarter, quarter)
+        partial[waves, :, columns] = jnp.dot(
+            mixed_ref[...], w_out_ref[:, columns], preferred_element_type=jnp.float32
+        ).astype(jnp.bfloat16)
+    pl.semaphore_wait(barrier, peers - 1 + 2)
+    sum_start(waves)
+
+    r = lax.broadcasted_iota(jnp.int32, (128, 128), 0)
+    c = lax.broadcasted_iota(jnp.int32, (128, 128), 1)
+    order[0] = (((r & 31) >> 2) * 16 + (r >> 5) * 4 + (r & 3) == c).astype(jnp.bfloat16)
+    order[1] = (((c & 31) >> 2) * 16 + (c >> 5) * 4 + (c & 3) == r).astype(jnp.bfloat16)
+    tall = peers * 16
+    r = lax.broadcasted_iota(jnp.int32, (tall, 128), 0)
+    c = lax.broadcasted_iota(jnp.int32, (tall, 128), 1)
+    place = (r >> 4) * 4 + (r & 3)
+    hit = (place == slot_row_ref[0:1, :]) | (place == slot_row_ref[1:2, :])
+    spread[...] = (hit & (((r >> 2) & 3) == (c >> 5))).astype(jnp.bfloat16)
+    r = lax.broadcasted_iota(jnp.int32, (128, tall), 0)
+    c = lax.broadcasted_iota(jnp.int32, (128, tall), 1)
+    place = (c >> 4) * 4 + (c & 3)
+    same = ((c >> 2) & 3) == (r >> 5)
+    share = jnp.where(same & (place == slot_col_ref[:, 0:1]), gate_col_ref[:, 0:1], 0.0) + jnp.where(
+        same & (place == slot_col_ref[:, 1:2]), gate_col_ref[:, 1:2], 0.0
+    )
+    coarse = share.astype(jnp.bfloat16)
+    weigh[0] = coarse
+    weigh[1] = (share - coarse.astype(jnp.float32)).astype(jnp.bfloat16)
+
+    sum_middle(waves)
+    left, right = sum_end(waves)
+    for first, part in ((0, left), (half, right)):
+        columns = pl.ds(first, half)
+        middle[:, columns] = (resid_ref[:, columns].astype(jnp.float32) + part).astype(jnp.bfloat16)
+    value = middle[...].astype(jnp.float32)
+    value = value * lax.rsqrt(jnp.mean(value * value, axis=1, keepdims=True) + 1e-06) * gain_ref[...]
+    value = value.astype(jnp.bfloat16)
+    for j in range(4):
+        stack[pl.ds(j * rows, rows), :] = value[:, j * quarter : (j + 1) * quarter]
+    outgoing[...] = jnp.dot(spread[...], stack[...], preferred_element_type=jnp.float32).astype(jnp.bfloat16)
+
+    def offsets(w):
+        last = w == waves - 1
+        far, close = half_ring - 1 - w, 1 + w
+        return (far, -far, jnp.where(last, half_ring, close), jnp.where(last, 0, -close))
+
+    def tile(x):
+        return pl.ds(pl.multiple_of(x * 16, 16), 16)
+
+    def dispatch(w, m, rel):
+        target = lax.rem(chip - offsets(w)[m] + 2 * chips, chips) * 2 + lax.rem(core + rel, 2)
+        return remote(
+            outgoing.at[tile(target), :],
+            inbox.at[w, tp, pl.ds((2 * m + rel) * 16, 16), :],
+            z_send,
+            z_recv.at[w, m // 2],
+            "sp",
+            target,
+        )
+
+    def answer(w, m, rel):
+        target = lax.rem(chip + offsets(w)[m] + chips, chips) * 2 + lax.rem(core + rel, 2)
+        return remote(
+            reply.at[w, pl.ds((2 * m + rel) * 16, 16), :],
+            returned.at[tile(me), :],
+            reply_send,
+            reply_recv,
+            "sp",
+            target,
+        )
+
+    def all_of(w, make):
+        for m in range(4):
+            for rel in range(2):
+                if m == 3 and rel == 0:
+
+                    @pl.when(w < waves - 1)
+                    def _():
+                        make(w, m, rel).start()
+
+                else:
+                    make(w, m, rel).start()
+
+    own_in = pltpu.make_async_copy(
+        outgoing.at[tile(me), :], inbox.at[waves - 1, tp, pl.ds(96, 16), :], self_sem.at[0]
+    )
+    own_out = pltpu.make_async_copy(
+        reply.at[waves - 1, pl.ds(96, 16), :], returned.at[tile(me), :], self_sem.at[1]
+    )
+    own_in.start()
+
+    def send_all(w, _):
+        all_of(w, dispatch)
+        return 0
+
+    lax.fori_loop(0, waves, send_all, 0)
+
+    def part(w, owner, h):
+        return inbox.at[w, owner, pl.ds(h * 64, 64), :]
+
+    def to_a(w, h, owner):
+        return remote(part(w, owner, h), part(w, owner, h), a_send.at[w, h], a_recv.at[w, h], "tp", peer_a)
+
+    def to_b(w, h, owner):
+        return remote(part(w, owner, h), part(w, owner, h), b_send.at[w, h], b_recv.at[w, h], "tp", peer_b)
+
+    def relay_a(w, owner):
+        return remote(part(w, owner, 0), part(w, owner, 0), relay_send.at[w, 0], relay_recv.at[w, 0], "tp", peer_a)
+
+    def relay_b(w, owner):
+        return remote(part(w, owner, 1), part(w, owner, 1), relay_send.at[w, 1], relay_recv.at[w, 1], "tp", peer_b)
+
+    def landed(w, h, count):
+        ref = inbox.at[w, tp, pl.ds(h * 64, count), :]
+        return remote(ref, ref, z_send, z_recv.at[w, h], "sp", lax.rem(me + 1, peers))
+
+    def forward(w):
+        landed(w, 0, 64).wait_recv()
+        to_a(w, 0, tp).start()
+        to_b(w, 0, tp).start()
+
+        @pl.when(w < waves - 1)
+        def _():
+            landed(w, 1, 64).wait_recv()
+
+        @pl.when(w == waves - 1)
+        def _():
+            landed(w, 1, 48).wait_recv()
+            own_in.wait()
+
+        to_a(w, 1, tp).start()
+        to_b(w, 1, tp).start()
+
+    def pass_on(w):
+        to_b(w, 0, peer_b).wait_recv()
+        relay_a(w, peer_b).start()
+        to_a(w, 1, peer_a).wait_recv()
+        relay_b(w, peer_a).start()
+
+    def compute(w):
+        to_a(w, 0, peer_a).wait_recv()
+        to_b(w, 1, peer_b).wait_recv()
+        relay_a(w, across).wait_recv()
+        relay_b(w, across).wait_recv()
+        for j in range(4):
+            turned = jnp.dot(order[0], inbox[w, j], preferred_element_type=jnp.float32).astype(jnp.bfloat16)
+            for k in range(4):
+                rows_in[pl.ds(j * 32, 32), pl.ds(k * quarter, quarter)] = turned[k * 32 : (k + 1) * 32]
+        gate = jnp.dot(rows_in[...], w_gate[...], preferred_element_type=jnp.float32)
+        lift = jnp.dot(rows_in[...], w_up[...], preferred_element_type=jnp.float32)
+        hidden = (gate / (1.0 + jnp.exp(-gate)) * lift).astype(jnp.bfloat16)
+        for j in range(4):
+            columns = pl.ds(j * quarter, quarter)
+            partial[w, :, columns] = jnp.dot(
+                hidden, w_down[:, columns], preferred_element_type=jnp.float32
+            ).astype(jnp.bfloat16)
+        sum_start(w)
+
+    def give_back(w):
+        left, right = sum_end(w)
+        left, right = left.astype(jnp.bfloat16), right.astype(jnp.bfloat16)
+        whole = jnp.concatenate(
+            [left[:, :quarter], left[:, quarter:], right[:, :quarter], right[:, quarter:]], axis=0
+        )
+        reply[w] = jnp.dot(order[1], whole, preferred_element_type=jnp.float32).astype(jnp.bfloat16)
+        all_of(w, answer)
+
+        @pl.when(w == waves - 1)
+        def _():
+            own_out.start()
+
+    for copy in loads:
+        copy.wait()
+
+    def turn(it, _):
+        @pl.when(it < waves)
+        def _():
+            forward(it)
+
+        @pl.when((it >= 2) & (it < waves + 2))
+        def _():
+            sum_middle(it - 2)
+
+        @pl.when((it >= 1) & (it < waves + 1))
+        def _():
+            compute(it - 1)
+
+        @pl.when(it < waves)
+        def _():
+            pass_on(it)
+
+        @pl.when((it >= 2) & (it < waves + 2))
+        def _():
+            give_back(it - 2)
+
+        return 0
+
+    lax.fori_loop(0, waves + 2, turn, 0)
+
+    rest = (peers - 1) * 16
+    own_out.wait()
+    everything = returned.at[pl.ds(0, rest), :]
+    remote(everything, everything, reply_send, reply_recv, "sp", lax.rem(me + 1, peers)).wait_recv()
+    mixed_rows = jnp.dot(weigh[0], returned[...], preferred_element_type=jnp.float32) + jnp.dot(
+        weigh[1], returned[...], preferred_element_type=jnp.float32
+    )
+    for j in range(4):
+        columns = pl.ds(j * quarter, quarter)
+        out_ref[:, columns] = (
+            middle[:, columns].astype(jnp.float32) + mixed_rows[j * rows : (j + 1) * rows]
+        ).astype(jnp.bfloat16)
+
+    sent = outgoing.at[pl.ds(0, rest), :]
+    remote(sent, sent, z_send, z_recv.at[0, 0], "sp", lax.rem(me + 1, peers)).wait_send()
+    remote(everything, everything, reply_send, reply_recv, "sp", lax.rem(me + 1, peers)).wait_send()
+
+    def drain(w, _):
+        for i in range(4):
+            first_send_of(w, i).wait_send()
+        for i in range(2):
+            second_send_of(w, i).wait_send()
+
+        @pl.when(w < waves)
+        def _():
+            for h in range(2):
+                to_a(w, h, tp).wait_send()
+                to_b(w, h, tp).wait_send()
+            relay_a(w, peer_b).wait_send()
+            relay_b(w, peer_a).wait_send()
+
+        return 0
+
+    lax.fori_loop(0, waves + 1, drain, 0)
+
+
+def feed(mixed, w_out, resid, norm_gain, expert_ids, expert_gates, w_gate, w_up, w_down, chips):
+    rows, width = resid.shape
+    quarter, half = width // 4, width // 2
+    peers = 2 * chips
+    waves = chips // 4
+    hidden = w_gate.shape[2]
+    flat = expert_ids.reshape(-1)
+    index = jnp.arange(flat.shape[0], dtype=jnp.int32)
+    rank = jnp.sum(
+        ((flat[:, None] == flat[None, :]) & (index[None, :] < index[:, None])).astype(jnp.int32), axis=1
+    )
+    slot = (flat * 4 + rank).reshape(rows, TOPK)
+    slot_col = jnp.tile(slot, (4, 1))
+    slot_row = slot_col.T
+    gate_col = jnp.tile(expert_gates, (4, 1))
+    vmem = pl.BlockSpec(memory_space=pltpu.VMEM)
+    hbm = pl.BlockSpec(memory_space=pl.ANY)
+    dma = pltpu.SemaphoreType.DMA
+    bf16 = jnp.bfloat16
+    return pl.pallas_call(
+        functools.partial(feed_kernel, chips),
+        out_shape=jax.ShapeDtypeStruct((rows, width), bf16),
+        in_specs=[vmem] * 7 + [hbm] * 3,
+        out_specs=vmem,
+        scratch_shapes=[
+            pltpu.VMEM((width, hidden), bf16),
+            pltpu.VMEM((width, hidden), bf16),
+            pltpu.VMEM((hidden, width), bf16),
+            pltpu.VMEM((waves + 1, 4 * rows, width), bf16),
+            pltpu.VMEM((waves + 1, 2, rows, half), bf16),
+            pltpu.VMEM((waves + 1, 2, rows, half), bf16),
+            pltpu.VMEM((waves + 1, 2, rows, half), bf16),
+            pltpu.VMEM((waves + 1, rows, half), bf16),
+            pltpu.VMEM((waves + 1, rows, half), bf16),
+            pltpu.VMEM((rows, width), bf16),
+            pltpu.VMEM((4 * rows, quarter), bf16),
+            pltpu.VMEM((peers * 16, quarter), bf16),
+            pltpu.VMEM((waves, 4, 128, quarter), bf16),
+            pltpu.VMEM((128, width), bf16),
+            pltpu.VMEM((waves, 128, quarter), bf16),
+            pltpu.VMEM((peers * 16, quarter), bf16),
+            pltpu.VMEM((2, 128, 128), bf16),
+            pltpu.VMEM((peers * 16, 128), bf16),
+            pltpu.VMEM((2, 128, peers * 16), bf16),
+            dma((3,)),
+            dma((2,)),
+            dma,
+            dma((waves, 2)),
+            dma((waves, 2)),
+            dma((waves, 2)),
+            dma((waves, 2)),
+            dma((waves, 2)),
+            dma((waves, 2)),
+            dma((waves, 2)),
+            dma((waves + 1, 4)),
+            dma((waves + 1, 4)),
+            dma((waves + 1, 2)),
+            dma((waves + 1, 2)),
+            dma,
+            dma,
+        ],
+        compiler_params=pltpu.CompilerParams(
+            collective_id=1, has_side_effects=True, vmem_limit_bytes=48 * 1024 * 1024
+        ),
+        name="feed",
+    )(mixed, w_out, resid, norm_gain.reshape(1, -1), slot_row, slot_col, gate_col, w_gate, w_up, w_down)
+
+
 def local(
     queries,
     keys,
@@ -369,50 +751,11 @@
     w_up,
     w_down,
 ):
-    sp_count = lax.axis_size("sp")
-    tp_count = lax.axis_size("tp")
-    mixed = attention(queries, keys, values, head_bias, documents, sp_count // 2)
-    projected = summed_on_arrival(
-        jnp.dot(mixed, w_out, preferred_element_type=jnp.float32).astype(jnp.bfloat16), "tp", 0
-    )
-    middle = (resid.astype(jnp.float32) + projected).astype(jnp.bfloat16)
-    middle_value = middle.astype(jnp.float32)
-    normed = (
-        middle_value
-        * lax.rsqrt(jnp.mean(middle_value * middle_value, axis=1, keepdims=True) + 1e-06)
-        * norm_gain
-    ).astype(jnp.bfloat16)
-    row_count = normed.shape[0]
-    expert_count = w_gate.shape[0] * sp_count
-    slot_limit = min(row_count, max(2, 2 * TOPK * row_count // expert_count))
-    flat_ids = expert_ids.reshape(-1)
-    onehot_ids = (flat_ids[:, None] == jnp.arange(expert_count, dtype=jnp.int32)[None, :]).astype(
-        jnp.int32
-    )
-    earlier = jnp.cumsum(onehot_ids, axis=0) - onehot_ids
-    slot_ids = jnp.sum(earlier * onehot_ids, axis=1)
-    target = flat_ids * slot_limit + slot_ids
-    placing = (
-        jnp.arange(expert_count * slot_limit, dtype=jnp.int32)[:, None] == target[None, :]
-    ).astype(jnp.bfloat16)
-    by_token = jnp.sum(placing.reshape(expert_count * slot_limit, row_count, TOPK), axis=2)
-    outgoing = jnp.dot(by_token, normed, preferred_element_type=jnp.float32).astype(jnp.bfloat16)
-    outgoing = outgoing.reshape(expert_count, slot_limit, D)
-    arrived = lax.all_to_all(outgoing, "sp", split_axis=0, concat_axis=0, tiled=True)
-    gathered = collect(arrived, "tp", 0)
-    expert_rows = gathered.reshape(-1, D)
-    gate_value = jnp.dot(expert_rows, w_gate[0], preferred_element_type=jnp.float32)
-    up_value = jnp.dot(expert_rows, w_up[0], preferred_element_type=jnp.float32)
-    hidden = (jax.nn.silu(gate_value) * up_value).astype(jnp.bfloat16)
-    partial_out = jnp.dot(hidden, w_down[0], preferred_element_type=jnp.float32)
-    summed = summed_on_arrival(
-        partial_out.reshape(tp_count, sp_count * slot_limit, D).astype(jnp.bfloat16), "tp", 0
-    )
-    expert_result = summed.reshape(sp_count, slot_limit, D).astype(jnp.bfloat16)
-    returned = lax.all_to_all(expert_result, "sp", split_axis=0, concat_axis=0, tiled=True)
-    routed = jnp.dot(placing.T, returned.reshape(-1, D), preferred_element_type=jnp.float32)
-    combined = jnp.sum(expert_gates[:, :, None] * routed.reshape(row_count, TOPK, D), axis=1)
-    return (middle_value + combined).astype(jnp.bfloat16)
+    chips = lax.axis_size("sp") // 2
+    mixed = attention(queries, keys, values, head_bias, documents, chips)
+    return feed(
+        mixed, w_out, resid, norm_gain, expert_ids, expert_gates, w_gate, w_up, w_down, chips
+    )
 
 
 def solution(mesh):

time: 247 us -> 153 us (0.62)
  blocking collectives: 99.3 us -> 0 us
  Pallas kernels: 60.7 us -> 141 us
  waiting for transfers between devices: 41.8 us -> 0 us
  matrix products: 13.5 us -> 0 us
  starting transfers between devices: 11.2 us -> 0 us
  other arithmetic: 6.24 us -> 1.53 us
  local copies, waits for them, and re-layouts: 12.8 us -> 9.9 us
    all_to_all x3 -> x0, blocking collectives: 99.3 us -> none  [the longest x1 42.1 us: local(): lax.all_to_all(outgoing, 'sp', split_axis=0, concat_axis=0, tiled=True)]
    pallas_call x0 -> x1, Pallas kernels: none -> 80.1 us  [feed(): pl.pallas_call(functools.partial(feed_kernel, chips), out_shape=jax.Shape...]
    all_to_all x2 -> x0, waiting for transfers between devices: 41.8 us -> none  [the longest x1 33.4 us: local(): lax.all_to_all(expert_result, 'sp', split_axis=0, concat_axis=0, tiled=True)]
    dot_general x6 -> x0, matrix products: 13.5 us -> none  [the longest x1 4.45 us: local(): jnp.dot(expert_rows, w_gate[0], preferred_element_type=jnp.float32)]
    all_to_all x2 -> x0, starting transfers between devices: 11.2 us -> none  [the longest x1 6.89 us: local(): lax.all_to_all(expert_result, 'sp', split_axis=0, concat_axis=0, tiled=True)]
    unnamed x15 -> x13, local copies, waits for them, and re-layouts: 0.12 us -> 8.15 us
    reduce_sum x5 -> x1, other arithmetic: 4.47 us -> 0.18 us  [feed(): jnp.sum(((flat[:, None] == flat[None, :]) & (index[None, :] < index[:, No...]
    reshape x3 -> x0, local copies, waits for them, and re-layouts: 4.12 us -> none  [the longest x1 2.05 us: local(): outgoing = outgoing.reshape(expert_count, slot_limit, D)]
  transfers between devices with their start and end apart: 2 -> 0, of which waited for: 2 -> 0; matrix products, arithmetic and copies ran while one was open for 0% -> 0% of each run, Pallas kernels for 0% -> 0%
where the time goes in v2:
time: 153 us; the launch traced here: 152 us
  Pallas kernels  141 us (92%)
  local copies, waits for them, and re-layouts  9.9 us (6%)
  other arithmetic  1.53 us (1%)
    pallas_call x1, Pallas kernels, feed(): pl.pallas_call(functools.partial(feed_kernel, chips), out_shape=jax.Shape...  80.1 us
    pallas_call x1, Pallas kernels, attention(): pl.pallas_call(functools.partial(attention_kernel, chips, reach), out_sha...  60.9 us
    unnamed x13, local copies, waits for them, and re-layouts  8.15 us

profile of v2, /device:TPU:33, one launch (start us, length us, event | category | flops | bytes accessed | tf_op | source)
XLA Modules:
  0.0 152.5 jit_solution(8461042355057547476)
XLA Ops:
  0.0 0.7 convert_element_type.6
  0.7 0.6 broadcast_in_dim.4.doc_row_ref
  1.3 0.8 copy.32
  2.0 0.8 copy.29
  2.8 0.1 eq.15
  2.9 0.2 convert_reduce_fusion
  3.1 0.1 reduce_sum.12
  3.2 0.1 copy.30
  3.3 0.7 multiply_add_fusion
  3.9 0.1 copy.31
  4.0 0.7 broadcast_in_dim.5.doc_col_ref
  4.7 0.1 copy.33.slot_row_ref
  4.8 60.9 %attention.1.mixed_ref = bf16[128,512]{1,0:T(8,128)(2,1)} custom-call(bf16[128,512]{1,0:T(8,128)(2,1)} %q_ref.1, bf16[128,256]{1,0:T(8,128)(2,1)} %k_ref.1, bf16[128,256]{1,0:T(8,128)(2,1)} %v_ref.1, bf16[16,128]{1,0:T(8,128)(2,1)} %broadcast_in_dim.4.doc_row_ref, bf16[128,128]{1,0:T(8,128)(2,1)} %broadcast_in_dim.5.doc_col_ref, f32[4]{0:T(128)} %bias_ref.1), custom_call_target="tpu_custom_call" | custom-call | tf_op jit(solution)/shard_map/attention/pallas_call | solution.py:275
  65.7 0.0 copy-start
  65.7 1.9 %copy-done = bf16[1,2048,768]{2,1,0:T(8,128)(2,1)S(1)} copy-done((bf16[1,2048,768]{2,1,0:T(8,128)(2,1)S(1)}, bf16[1,2048,768]{2,1,0:T(8,128)(2,1)}, u32[]{:S(2)}) %copy-start) | copy-done | bytes 3145752
  67.6 0.0 copy-start.1
  67.6 1.6 %copy-done.1 = bf16[512,2048]{1,0:T(8,128)(2,1)S(1)} copy-done((bf16[512,2048]{1,0:T(8,128)(2,1)S(1)}, bf16[512,2048]{1,0:T(8,128)(2,1)}, u32[]{:S(2)}) %copy-start.1) | copy-done | bytes 2097176
  69.2 0.0 copy-start.2
  69.2 0.9 copy-done.2
  70.1 0.0 copy-start.3
  70.1 0.9 copy-done.3
  71.0 0.0 copy-start.4
  71.0 0.7 copy-done.4
  71.7 80.1 %feed.1 = bf16[32,2048]{1,0:T(8,128)(2,1)S(1)} custom-call(bf16[128,512]{1,0:T(8,128)(2,1)S(1)} %copy-done.2, bf16[512,2048]{1,0:T(8,128)(2,1)S(1)} %copy-done.1, bf16[32,2048]{1,0:T(8,128)(2,1)S(1)} %copy-done.3, f32[1,2048]{1,0:T(1,128)S(1)} %bitcast.8, s32[2,128]{1,0:T(2,128)S(1)} %copy.33.slot_row_ref, s32[128,2]{1,0:T(8,128)S(1)} %bitcast.6, ...), custom_call_target="tpu_custom_call" | custom-call | tf_op jit(solution)/shard_map/feed/pallas_call | solution.py:690
  151.8 0.7 copy.35
  (2 shorter events, 0.0 us)
Async XLA Ops:
  65.7 1.9 %copy-start = (bf16[1,2048,768]{2,1,0:T(8,128)(2,1)S(1)}, bf16[1,2048,768]{2,1,0:T(8,128)(2,1)}, u32[]{:S(2)}) copy-start(bf16[1,2048,768]{2,1,0:T(8,128)(2,1)} %w_gate_hbm.1) | copy-start | bytes 9437188
  67.6 1.6 %copy-start.1 = (bf16[512,2048]{1,0:T(8,128)(2,1)S(1)}, bf16[512,2048]{1,0:T(8,128)(2,1)}, u32[]{:S(2)}) copy-start(bf16[512,2048]{1,0:T(8,128)(2,1)} %w_out_ref.1) | copy-start | bytes 6291460
  69.2 0.9 copy-start.2
  70.1 0.9 copy-start.3
  71.0 0.7 copy-start.4

commit v3 on v2

--- a/solution.py
+++ b/solution.py
@@ -7,12 +7,6 @@
 from jax.experimental import pallas as pl
 from jax.experimental.pallas import tpu as pltpu
 from jax.sharding import PartitionSpec as P
-
-TOPK = 2
-SP = "sp"
-GRP_SP = ("grp", "sp")
-GRP_SP_TP = ("grp", "sp", "tp")
-
 
 MESH_ID = pl.DeviceIdType.MESH
 LOG2E = math.log2(math.e)
@@ -29,25 +23,33 @@
     )
 
 
-def attention_kernel(
+def layer_kernel(
     chips,
     reach,
     q_ref,
     k_ref,
     v_ref,
-    doc_row_ref,
-    doc_col_ref,
+    w_out_hbm,
+    resid_hbm,
+    w_gate_hbm,
+    w_up_hbm,
+    w_down_hbm,
+    doc_ref,
+    gain_ref,
+    ids_ref,
+    gates_ref,
     bias_ref,
     out_ref,
     kv,
     qx,
+    doc_rows_own,
     doc_col,
     tri,
     near,
     far,
     carry,
     mix,
-    mixed_in,
+    mixed,
     pair_send,
     pair_recv,
     own_sem,
@@ -57,10 +59,49 @@
     down_recv,
     back_send,
     back_recv,
+    w_out,
+    w_gate,
+    w_up,
+    w_down,
+    resid,
+    partial,
+    first_a,
+    first_b,
+    summed,
+    second_a,
+    second_b,
+    middle,
+    stack,
+    outgoing,
+    inbox,
+    rows_in,
+    reply,
+    returned,
+    order,
+    spread,
+    weigh,
+    lines,
+    weight_sem,
+    self_sem,
+    z_send,
+    z_recv,
+    a_send,
+    a_recv,
+    b_send,
+    b_recv,
+    relay_send,
+    relay_recv,
+    first_send,
+    first_recv,
+    second_send,
+    second_recv,
+    reply_send,
+    reply_recv,
 ):
     tok = q_ref.shape[0]
     both = 2 * tok
     me = lax.axis_index("sp")
+    tp = lax.axis_index("tp")
     chip = me // 2
     core = me % 2
     other = 1 - core
@@ -70,37 +111,56 @@
     up_steps = chips // 2
     down_steps = chips - 1 - up_steps
 
+    peer_a = tp + 1 - 2 * (tp % 2)
+    peer_b = 3 - tp
+    across = lax.rem(tp + 2, 4)
+
     barrier = pltpu.get_barrier_semaphore()
     for peer in (partner, up, down):
         pl.semaphore_signal(barrier, inc=1, device_id={"sp": peer}, device_id_type=MESH_ID)
+    for peer in (peer_a, peer_b):
+        pl.semaphore_signal(barrier, inc=1, device_id={"tp": peer}, device_id_type=MESH_ID)
 
     def at(x, size=None):
         return pl.ds(pl.multiple_of(x, 128), size or tok)
 
-    doc_rows = doc_row_ref.shape[0]
+    doc_rows = doc_rows_own.shape[0]
     rows_here = at(core * tok)
-    moves = []
+    moves = [
+        (lambda o: k_ref.at[:, at(o * 128, 128)], kv.at[chip, rows_here, :]),
+        (lambda o: v_ref.at[:, at(o * 128, 128)], kv.at[chip, at(both + core * tok), :]),
+        (
+            lambda o: doc_rows_own,
+            kv.at[chip, pl.ds(pl.multiple_of(2 * both + core * doc_rows, doc_rows), doc_rows), :],
+        ),
+    ]
     for h in range(2):
         moves.append((lambda o, h=h: q_ref.at[:, at(o * 256 + h * 128, 128)], qx.at[at(h * both + core * tok), :]))
-    moves.append((lambda o: k_ref.at[:, at(o * 128, 128)], kv.at[chip, rows_here, :]))
-    moves.append((lambda o: v_ref.at[:, at(o * 128, 128)], kv.at[chip, at(both + core * tok), :]))
-    moves.append(
-        (
-            lambda o: doc_row_ref,
-            kv.at[chip, pl.ds(pl.multiple_of(2 * both + core * doc_rows, doc_rows), doc_rows), :],
-        )
-    )
-    moves.append((lambda o: doc_col_ref, doc_col.at[rows_here, :]))
+    doc_rows_own[...] = jnp.broadcast_to(doc_ref[...].astype(jnp.float32), (doc_rows, tok)).astype(jnp.bfloat16)
     kept = [pltpu.make_async_copy(src(core), dst, own_sem.at[i]) for i, (src, dst) in enumerate(moves)]
     for copy in kept:
         copy.start()
-    pl.semaphore_wait(barrier, 3)
+    pl.semaphore_wait(barrier, 5)
     traded = [
         remote(src(other), dst, pair_send.at[i], pair_recv.at[i], "sp", partner)
         for i, (src, dst) in enumerate(moves)
     ]
-    for i in (2, 3, 4, 0, 1, 5):
-        traded[i].start()
+    for copy in traded:
+        copy.start()
+    loads = [
+        pltpu.make_async_copy(src, dst, weight_sem.at[i])
+        for i, (src, dst) in enumerate(
+            (
+                (w_out_hbm, w_out),
+                (resid_hbm, resid),
+                (w_gate_hbm.at[0], w_gate),
+                (w_up_hbm.at[0], w_up),
+                (w_down_hbm.at[0], w_down),
+            )
+        )
+    ]
+    for copy in loads:
+        copy.start()
     row_id = lax.broadcasted_iota(jnp.int32, (both, both), 0)
     col_id = lax.broadcasted_iota(jnp.int32, (both, both), 1)
     tri[...] = (row_id > col_id).astype(jnp.bfloat16)
@@ -108,6 +168,58 @@
     far[...] = jnp.zeros_like(far)
     carry[...] = jnp.zeros_like(carry)
 
+    peers = 2 * chips
+    rows = resid.shape[0]
+    r = lax.broadcasted_iota(jnp.int32, (128, 128), 0)
+    c = lax.broadcasted_iota(jnp.int32, (128, 128), 1)
+    order[0] = (((r & 31) >> 2) * 16 + (r >> 5) * 4 + (r & 3) == c).astype(jnp.bfloat16)
+    order[1] = (((c & 31) >> 2) * 16 + (c >> 5) * 4 + (c & 3) == r).astype(jnp.bfloat16)
+    lines[...] = jnp.zeros_like(lines)
+    lines[0:2, 0:rows] = ids_ref[...].astype(jnp.float32)
+    lines[2:4, 0:rows] = gates_ref[...]
+    tiled = lines[...]
+    tiled = tiled + pltpu.roll(tiled, rows, 1)
+    tiled = tiled + pltpu.roll(tiled, 2 * rows, 1)
+    first_there, second_there, first_gate, second_gate = (
+        jnp.broadcast_to(tiled[k : k + 1], (128, 128)) for k in range(4)
+    )
+    first_here, second_here, first_gate, second_gate = (
+        x.T for x in (first_there, second_there, first_gate, second_gate)
+    )
+    once = c < rows
+    before = once & (c < (r & (rows - 1)))
+
+    def count(found):
+        return jnp.sum(found.astype(jnp.float32), axis=1, keepdims=True)
+
+    first_slot = first_here[:, 0:1] * 4.0 + count(before & (first_here == first_there))
+    second_slot = (
+        second_here[:, 0:1] * 4.0
+        + count(once & (second_here == first_there))
+        + count(before & (second_here == second_there))
+    )
+    first_line = jnp.broadcast_to(first_slot, (128, 128)).T[0:1].astype(jnp.int32)
+    second_line = jnp.broadcast_to(second_slot, (128, 128)).T[0:1].astype(jnp.int32)
+    first_slot = first_slot.astype(jnp.int32)
+    second_slot = second_slot.astype(jnp.int32)
+    tall = peers * 16
+    r = lax.broadcasted_iota(jnp.int32, (tall, 128), 0)
+    c = lax.broadcasted_iota(jnp.int32, (tall, 128), 1)
+    place = (r >> 4) * 4 + (r & 3)
+    hit = (place == first_line) | (place == second_line)
+    spread[...] = (hit & (((r >> 2) & 3) == (c >> 5))).astype(jnp.bfloat16)
+    r = lax.broadcasted_iota(jnp.int32, (128, tall), 0)
+    c = lax.broadcasted_iota(jnp.int32, (128, tall), 1)
+    place = (c >> 4) * 4 + (c & 3)
+    same = ((c >> 2) & 3) == (r >> 5)
+    share = jnp.where(same & (place == first_slot), first_gate[:, 0:1], 0.0) + jnp.where(
+        same & (place == second_slot), second_gate[:, 0:1], 0.0
+    )
+    coarse = share.astype(jnp.bfloat16)
+    weigh[0] = coarse
+    weigh[1] = (share - coarse.astype(jnp.float32)).astype(jnp.bfloat16)
+
+
     pieces = ((0, both), (both, both + 2 * doc_rows))
 
     def upward(step, piece):
@@ -134,18 +246,21 @@
         ref = kv.at[block, pl.ds(first, count), :]
         return remote(ref, ref, down_send.at[step, piece], down_recv.at[step, piece], "sp", down)
 
-    for i in (2, 3, 4):
-        kept[i].wait()
-    traded[2].wait_recv()
+    kept[0].wait()
+    traded[0].wait_recv()
     upward(0, 0).start()
     downward(0, 0).start()
-    traded[3].wait_recv()
-    traded[4].wait_recv()
+    for i in (1, 2):
+        kept[i].wait()
+        traded[i].wait_recv()
     upward(0, 1).start()
     downward(0, 1).start()
-    for i in (0, 1, 5):
+    for i in (3, 4):
         kept[i].wait()
         traded[i].wait_recv()
+    for i in range(2):
+        line = kv[chip, 2 * both + i * doc_rows : 2 * both + (i + 1) * doc_rows, :].astype(jnp.float32)
+        doc_col[i * tok : (i + 1) * tok, :] = jnp.broadcast_to(line[0:1], (tok, tok)).T
 
     scale = LOG2E / math.sqrt(128.0)
 
@@ -162,7 +277,7 @@
         tail = jnp.log(1.0 + jnp.exp2(-jnp.abs(logits))) * LOG2E
         spend = jnp.maximum(logits, 0.0) + tail
         gain = jnp.minimum(logits, 0.0) - tail
-        doc_here = doc_col[pl.ds(first, tok), :].astype(jnp.float32)
+        doc_here = doc_col[pl.ds(first, tok), :]
         doc_here = jnp.concatenate([doc_here, doc_here], axis=1)
         low = kv[block, 2 * both : 2 * both + doc_rows, :].astype(jnp.float32)
         high = kv[block, 2 * both + doc_rows : 2 * both + 2 * doc_rows, :].astype(jnp.float32)
@@ -226,164 +341,26 @@
     for h in range(2):
         rows = pl.ds(h * both, both)
         mix[h] = (near[rows, :] + jnp.exp2(-carry[rows, :]) * far[rows, :]).astype(jnp.bfloat16)
+    def mixed_at(h):
+        return mixed.at[:, at(core * 256 + h * 128, 128)]
+
     back = [
-        remote(
-            mix.at[h, at(other * tok), :],
-            mixed_in.at[h],
-            back_send.at[h],
-            back_recv.at[h],
-            "sp",
-            partner,
-        )
+        remote(mix.at[h, at(other * tok), :], mixed_at(h), back_send.at[h], back_recv.at[h], "sp", partner)
         for h in range(2)
     ]
     for copy in back:
         copy.start()
     for h in range(2):
-        out_ref[:, at(core * 256 + h * 128, 128)] = mix[h, at(core * tok), :]
-    for h in range(2):
-        back[h].wait_recv()
-        out_ref[:, at(other * 256 + h * 128, 128)] = mixed_in[h]
-    for copy in traded + back:
-        copy.wait_send()
-
-    def drain(step, _):
-        for piece in range(2):
-            upward(step, piece).wait_send()
-
-            @pl.when(step < down_steps)
-            def _():
-                downward(step, piece).wait_send()
-
-        return 0
-
-    lax.fori_loop(0, up_steps, drain, 0)
-
-
-def attention(queries, keys, values, head_bias, documents, chips):
-    tok = queries.shape[0]
-    both = 2 * tok
-    doc = documents.astype(jnp.bfloat16)
-    doc_rows = 16
-    doc_row = jnp.broadcast_to(doc[None, :], (doc_rows, tok))
-    doc_col = jnp.broadcast_to(doc[:, None], (tok, 128))
-    longest = chips * both * 3 // 4
-    reach = (longest - 1 + both - 1) // both
-    up_steps = chips // 2
-    vmem = pl.BlockSpec(memory_space=pltpu.VMEM)
-    dma = pltpu.SemaphoreType.DMA
-    return pl.pallas_call(
-        functools.partial(attention_kernel, chips, reach),
-        out_shape=jax.ShapeDtypeStruct((tok, 512), jnp.bfloat16),
-        in_specs=[vmem] * 5 + [pl.BlockSpec(memory_space=pltpu.SMEM)],
-        out_specs=vmem,
-        scratch_shapes=[
-            pltpu.VMEM((chips, 2 * both + 2 * doc_rows, 128), jnp.bfloat16),
-            pltpu.VMEM((2 * both, 128), jnp.bfloat16),
-            pltpu.VMEM((both, 128), jnp.bfloat16),
-            pltpu.VMEM((both, both), jnp.bfloat16),
-            pltpu.VMEM((2 * both, 128), jnp.float32),
-            pltpu.VMEM((2 * both, 128), jnp.float32),
-            pltpu.VMEM((2 * both, 128), jnp.float32),
-            pltpu.VMEM((2, both, 128), jnp.bfloat16),
-            pltpu.VMEM((2, tok, 128), jnp.bfloat16),
-            dma((6,)),
-            dma((6,)),
-            dma((6,)),
-            dma((up_steps, 2)),
-            dma((up_steps, 2)),
-            dma((up_steps, 2)),
-            dma((up_steps, 2)),
-            dma((2,)),
-            dma((2,)),
-        ],
-        compiler_params=pltpu.CompilerParams(collective_id=0, has_side_effects=True),
-        name="attention",
-    )(queries, keys, values, doc_row, doc_col, head_bias)
-
-
-def feed_kernel(
-    chips,
-    mixed_ref,
-    w_out_ref,
-    resid_ref,
-    gain_ref,
-    slot_row_ref,
-    slot_col_ref,
-    gate_col_ref,
-    w_gate_hbm,
-    w_up_hbm,
-    w_down_hbm,
-    out_ref,
-    w_gate,
-    w_up,
-    w_down,
-    partial,
-    first_a,
-    first_b,
-    summed,
-    second_a,
-    second_b,
-    middle,
-    stack,
-    outgoing,
-    inbox,
-    rows_in,
-    reply,
-    returned,
-    order,
-    spread,
-    weigh,
-    weight_sem,
-    self_sem,
-    z_send,
-    z_recv,
-    a_send,
-    a_recv,
-    b_send,
-    b_recv,
-    relay_send,
-    relay_recv,
-    first_send,
-    first_recv,
-    second_send,
-    second_recv,
-    reply_send,
-    reply_recv,
-):
+        mixed[:, at(core * 256 + h * 128, 128)] = mix[h, at(core * tok), :]
+    for copy in back:
+        copy.wait_recv()
+
     waves = chips // 4
     half_ring = chips // 2
     peers = 2 * chips
-    rows, width = resid_ref.shape
+    rows, width = resid.shape
     quarter = width // 4
     half = width // 2
-    me = lax.axis_index("sp")
-    tp = lax.axis_index("tp")
-    chip = me // 2
-    core = me % 2
-    low = tp % 2
-    peer_a = tp + 1 - 2 * low
-    peer_b = 3 - tp
-    across = lax.rem(tp + 2, 4)
-
-    loads = [
-        pltpu.make_async_copy(src.at[0], dst, weight_sem.at[i])
-        for i, (src, dst) in enumerate(((w_gate_hbm, w_gate), (w_up_hbm, w_up), (w_down_hbm, w_down)))
-    ]
-    for copy in loads:
-        copy.start()
-
-    barrier = pltpu.get_barrier_semaphore()
-
-    def greet(k, _):
-        pl.semaphore_signal(
-            barrier, inc=1, device_id={"sp": lax.rem(me + k, peers)}, device_id_type=MESH_ID
-        )
-        return 0
-
-    lax.fori_loop(1, peers, greet, 0)
-    for peer in (peer_a, peer_b):
-        pl.semaphore_signal(barrier, inc=1, device_id={"tp": peer}, device_id_type=MESH_ID)
 
     def block(n, which, first=0, size=None):
         return partial.at[n, pl.ds(pl.multiple_of(which * rows, rows), rows), pl.ds(first, size or width)]
@@ -433,40 +410,20 @@
         right = right + second_a[n].astype(jnp.float32)
         return left, right
 
+    for copy in loads:
+        copy.wait()
     for j in range(4):
         columns = pl.ds(j * quarter, quarter)
         partial[waves, :, columns] = jnp.dot(
-            mixed_ref[...], w_out_ref[:, columns], preferred_element_type=jnp.float32
+            mixed[...], w_out[:, columns], preferred_element_type=jnp.float32
         ).astype(jnp.bfloat16)
-    pl.semaphore_wait(barrier, peers - 1 + 2)
     sum_start(waves)
-
-    r = lax.broadcasted_iota(jnp.int32, (128, 128), 0)
-    c = lax.broadcasted_iota(jnp.int32, (128, 128), 1)
-    order[0] = (((r & 31) >> 2) * 16 + (r >> 5) * 4 + (r & 3) == c).astype(jnp.bfloat16)
-    order[1] = (((c & 31) >> 2) * 16 + (c >> 5) * 4 + (c & 3) == r).astype(jnp.bfloat16)
-    tall = peers * 16
-    r = lax.broadcasted_iota(jnp.int32, (tall, 128), 0)
-    c = lax.broadcasted_iota(jnp.int32, (tall, 128), 1)
-    place = (r >> 4) * 4 + (r & 3)
-    hit = (place == slot_row_ref[0:1, :]) | (place == slot_row_ref[1:2, :])
-    spread[...] = (hit & (((r >> 2) & 3) == (c >> 5))).astype(jnp.bfloat16)
-    r = lax.broadcasted_iota(jnp.int32, (128, tall), 0)
-    c = lax.broadcasted_iota(jnp.int32, (128, tall), 1)
-    place = (c >> 4) * 4 + (c & 3)
-    same = ((c >> 2) & 3) == (r >> 5)
-    share = jnp.where(same & (place == slot_col_ref[:, 0:1]), gate_col_ref[:, 0:1], 0.0) + jnp.where(
-        same & (place == slot_col_ref[:, 1:2]), gate_col_ref[:, 1:2], 0.0
-    )
-    coarse = share.astype(jnp.bfloat16)
-    weigh[0] = coarse
-    weigh[1] = (share - coarse.astype(jnp.float32)).astype(jnp.bfloat16)
 
     sum_middle(waves)
     left, right = sum_end(waves)
     for first, part in ((0, left), (half, right)):
         columns = pl.ds(first, half)
-        middle[:, columns] = (resid_ref[:, columns].astype(jnp.float32) + part).astype(jnp.bfloat16)
+        middle[:, columns] = (resid[:, columns].astype(jnp.float32) + part).astype(jnp.bfloat16)
     value = middle[...].astype(jnp.float32)
     value = value * lax.rsqrt(jnp.mean(value * value, axis=1, keepdims=True) + 1e-06) * gain_ref[...]
     value = value.astype(jnp.bfloat16)
@@ -604,9 +561,6 @@
         def _():
             own_out.start()
 
-    for copy in loads:
-        copy.wait()
-
     def turn(it, _):
         @pl.when(it < waves)
         def _():
@@ -666,36 +620,84 @@
         return 0
 
     lax.fori_loop(0, waves + 1, drain, 0)
-
-
-def feed(mixed, w_out, resid, norm_gain, expert_ids, expert_gates, w_gate, w_up, w_down, chips):
+    for copy in traded + back:
+        copy.wait_send()
+
+    def drain_ring(step, _):
+        for piece in range(2):
+            upward(step, piece).wait_send()
+
+            @pl.when(step < down_steps)
+            def _():
+                downward(step, piece).wait_send()
+
+        return 0
+
+    lax.fori_loop(0, up_steps, drain_ring, 0)
+
+
+def layer(
+    queries,
+    keys,
+    values,
+    head_bias,
+    documents,
+    w_out,
+    resid,
+    norm_gain,
+    expert_ids,
+    expert_gates,
+    w_gate,
+    w_up,
+    w_down,
+):
+    chips = lax.axis_size("sp") // 2
+    tok = queries.shape[0]
+    both = 2 * tok
+    doc_rows = 16
+    longest = chips * both * 3 // 4
+    reach = (longest - 1 + both - 1) // both
+    up_steps = chips // 2
     rows, width = resid.shape
     quarter, half = width // 4, width // 2
     peers = 2 * chips
     waves = chips // 4
     hidden = w_gate.shape[2]
-    flat = expert_ids.reshape(-1)
-    index = jnp.arange(flat.shape[0], dtype=jnp.int32)
-    rank = jnp.sum(
-        ((flat[:, None] == flat[None, :]) & (index[None, :] < index[:, None])).astype(jnp.int32), axis=1
-    )
-    slot = (flat * 4 + rank).reshape(rows, TOPK)
-    slot_col = jnp.tile(slot, (4, 1))
-    slot_row = slot_col.T
-    gate_col = jnp.tile(expert_gates, (4, 1))
+    smem = pl.BlockSpec(memory_space=pltpu.SMEM)
     vmem = pl.BlockSpec(memory_space=pltpu.VMEM)
     hbm = pl.BlockSpec(memory_space=pl.ANY)
     dma = pltpu.SemaphoreType.DMA
-    bf16 = jnp.bfloat16
+    bf16, f32 = jnp.bfloat16, jnp.float32
     return pl.pallas_call(
-        functools.partial(feed_kernel, chips),
+        functools.partial(layer_kernel, chips, reach),
         out_shape=jax.ShapeDtypeStruct((rows, width), bf16),
-        in_specs=[vmem] * 7 + [hbm] * 3,
+        in_specs=[hbm] * 8 + [vmem] * 4 + [smem],
         out_specs=vmem,
         scratch_shapes=[
+            pltpu.VMEM((chips, 2 * both + 2 * doc_rows, 128), bf16),
+            pltpu.VMEM((2 * both, 128), bf16),
+            pltpu.VMEM((doc_rows, tok), bf16),
+            pltpu.VMEM((both, 128), f32),
+            pltpu.VMEM((both, both), bf16),
+            pltpu.VMEM((2 * both, 128), f32),
+            pltpu.VMEM((2 * both, 128), f32),
+            pltpu.VMEM((2 * both, 128), f32),
+            pltpu.VMEM((2, both, 128), bf16),
+            pltpu.VMEM((tok, 512), bf16),
+            dma((5,)),
+            dma((5,)),
+            dma((5,)),
+            dma((up_steps, 2)),
+            dma((up_steps, 2)),
+            dma((up_steps, 2)),
+            dma((up_steps, 2)),
+            dma((2,)),
+            dma((2,)),
+            pltpu.VMEM(w_out.shape, bf16),
             pltpu.VMEM((width, hidden), bf16),
             pltpu.VMEM((width, hidden), bf16),
             pltpu.VMEM((hidden, width), bf16),
+            pltpu.VMEM((rows, width), bf16),
             pltpu.VMEM((waves + 1, 4 * rows, width), bf16),
             pltpu.VMEM((waves + 1, 2, rows, half), bf16),
             pltpu.VMEM((waves + 1, 2, rows, half), bf16),
@@ -712,7 +714,8 @@
             pltpu.VMEM((2, 128, 128), bf16),
             pltpu.VMEM((peers * 16, 128), bf16),
             pltpu.VMEM((2, 128, peers * 16), bf16),
-            dma((3,)),
+            pltpu.VMEM((8, 128), f32),
+            dma((5,)),
             dma((2,)),
             dma,
             dma((waves, 2)),
@@ -729,50 +732,40 @@
             dma,
             dma,
         ],
-        compiler_params=pltpu.CompilerParams(
-            collective_id=1, has_side_effects=True, vmem_limit_bytes=48 * 1024 * 1024
-        ),
-        name="feed",
-    )(mixed, w_out, resid, norm_gain.reshape(1, -1), slot_row, slot_col, gate_col, w_gate, w_up, w_down)
-
-
-def local(
-    queries,
-    keys,
-    values,
-    head_bias,
-    documents,
-    w_out,
-    resid,
-    norm_gain,
-    expert_ids,
-    expert_gates,
-    w_gate,
-    w_up,
-    w_down,
-):
-    chips = lax.axis_size("sp") // 2
-    mixed = attention(queries, keys, values, head_bias, documents, chips)
-    return feed(
-        mixed, w_out, resid, norm_gain, expert_ids, expert_gates, w_gate, w_up, w_down, chips
+        compiler_params=pltpu.CompilerParams(collective_id=0, has_side_effects=True),
+        name="layer",
+    )(
+        queries,
+        keys,
+        values,
+        w_out,
+        resid,
+        w_gate,
+        w_up,
+        w_down,
+        documents.reshape(1, -1),
+        norm_gain.reshape(1, -1),
+        expert_ids.T,
+        expert_gates.T,
+        head_bias,
     )
 
 
 def solution(mesh):
+    everyone = ("grp", "sp", "tp")
     in_specs = (
-        P(GRP_SP, "tp"),
-        P(GRP_SP, "tp"),
-        P(GRP_SP, "tp"),
+        P(("grp", "sp"), "tp"),
+        P(("grp", "sp"), "tp"),
+        P(("grp", "sp"), "tp"),
         P("tp"),
-        P(GRP_SP),
+        P(("grp", "sp")),
         P("tp", None),
-        P(GRP_SP_TP, None),
+        P(everyone, None),
         P(),
-        P(GRP_SP_TP, None),
-        P(GRP_SP_TP, None),
-        P(SP, None, "tp"),
-        P(SP, None, "tp"),
-        P(SP, "tp", None),
-    )
-    out_specs = P(GRP_SP_TP, None)
-    return jax.shard_map(local, mesh=mesh, in_specs=in_specs, out_specs=out_specs, check_vma=False)
+        P(everyone, None),
+        P(everyone, None),
+        P("sp", None, "tp"),
+        P("sp", None, "tp"),
+        P("sp", "tp", None),
+    )
+    return jax.shard_map(layer, mesh=mesh, in_specs=in_specs, out_specs=P(everyone, None), check_vma=False)

time: 153 us -> 137 us (0.90)
  local copies, waits for them, and re-layouts: 9.9 us -> 1.57 us
  Pallas kernels: 141 us -> 135 us
  other arithmetic: 1.53 us -> 0 us
    unnamed x13 -> x1, local copies, waits for them, and re-layouts: 8.15 us -> 1.57 us
    pallas_call x2 -> x1, Pallas kernels: 141 us -> 135 us  [layer(): pl.pallas_call(functools.partial(layer_kernel, chips, reach), out_shape=j...]
where the time goes in v3:
time: 137 us
  Pallas kernels  135 us (99%)
  local copies, waits for them, and re-layouts  1.57 us (1%)
    pallas_call x1, Pallas kernels, layer(): pl.pallas_call(functools.partial(layer_kernel, chips, reach), out_shape=j...  135 us

profile of v3, /device:TPU:33, one launch (start us, length us, event | category | flops | bytes accessed | tf_op | source)
XLA Modules:
  0.0 136.5 jit_solution(6338347937520721475)
XLA Ops:
  0.0 134.9 %layer.1 = bf16[32,2048]{1,0:T(8,128)(2,1)} custom-call(bf16[128,512]{1,0:T(8,128)(2,1)} %q_ref.1, bf16[128,256]{1,0:T(8,128)(2,1)} %k_ref.1, bf16[128,256]{1,0:T(8,128)(2,1)} %v_ref.1, bf16[512,2048]{1,0:T(8,128)(2,1)} %w_out_hbm.1, bf16[32,2048]{1,0:T(8,128)(2,1)} %resid_hbm.1, bf16[1,2048,768]{2,1,0:T(8,128)(2,1)} %w_gate_hbm.1, ...), custom_call_target="tpu_custom_call" | custom-call | tf_op jit(solution)/shard_map/layer/pallas_call | solution.py:671
  135.0 1.6 %copy.15 = bf16[32,2048]{1,0:T(8,128)(2,1)} copy(bf16[32,2048]{1,0:T(8,128)(2,1)} %layer.1) | data formatting | bytes 262144

commit v4 on v3

--- a/solution.py
+++ b/solution.py
@@ -50,6 +50,7 @@
     carry,
     mix,
     mixed,
+    known,
     pair_send,
     pair_recv,
     own_sem,
@@ -108,8 +109,26 @@
     partner = chip * 2 + other
     up = lax.rem(chip + 1, chips) * 2 + core
     down = lax.rem(chip + chips - 1, chips) * 2 + core
-    up_steps = chips // 2
-    down_steps = chips - 1 - up_steps
+    steps = chips // 2
+    hi = steps - 2
+    up_count = jnp.minimum(chip, steps)
+
+    def need_up(c, b):
+        return (c < chips) & (b >= c - steps)
+
+    def need_down(c, b):
+        return (b <= hi) & (b != c) & (lax.rem(b - c + chips, chips) < steps)
+
+    def up_block(k):
+        return chip - 1 - k
+
+    def down_block(k):
+        return lax.rem(chip + 1 + k, chips)
+
+    def comes_down(k):
+        return (k < steps - 1) & (down_block(k) <= hi)
+
+    below = lax.rem(chip + chips - 1, chips)
 
     peer_a = tp + 1 - 2 * (tp % 2)
     peer_b = 3 - tp
@@ -147,6 +166,18 @@
     ]
     for copy in traded:
         copy.start()
+
+    def tell(level):
+        for step in (1 << level, chips - (1 << level)):
+            pl.semaphore_signal(
+                known.at[level],
+                inc=1,
+                device_id={"sp": lax.rem(chip + step, chips) * 2 + core},
+                device_id_type=MESH_ID,
+            )
+
+    levels = (chips // 4).bit_length()
+    tell(0)
     loads = [
         pltpu.make_async_copy(src, dst, weight_sem.at[i])
         for i, (src, dst) in enumerate(
@@ -189,14 +220,14 @@
     once = c < rows
     before = once & (c < (r & (rows - 1)))
 
-    def count(found):
+    def tally(found):
         return jnp.sum(found.astype(jnp.float32), axis=1, keepdims=True)
 
-    first_slot = first_here[:, 0:1] * 4.0 + count(before & (first_here == first_there))
+    first_slot = first_here[:, 0:1] * 4.0 + tally(before & (first_here == first_there))
     second_slot = (
         second_here[:, 0:1] * 4.0
-        + count(once & (second_here == first_there))
-        + count(before & (second_here == second_there))
+        + tally(once & (second_here == first_there))
+        + tally(before & (second_here == second_there))
     )
     first_line = jnp.broadcast_to(first_slot, (128, 128)).T[0:1].astype(jnp.int32)
     second_line = jnp.broadcast_to(second_slot, (128, 128)).T[0:1].astype(jnp.int32)
@@ -220,41 +251,41 @@
     weigh[1] = (share - coarse.astype(jnp.float32)).astype(jnp.bfloat16)
 
 
+    count = 2
     pieces = ((0, both), (both, both + 2 * doc_rows))
 
-    def upward(step, piece):
-        block = lax.rem(chip - step + chips, chips)
-        first, count = pieces[piece]
-        ref = kv.at[block, pl.ds(first, count), :]
-        return remote(ref, ref, up_send.at[step, piece], up_recv.at[step, piece], "sp", up)
-
-    def downward(step, piece):
-        block = lax.rem(chip + step, chips)
-        first, count = pieces[piece]
-        ref = kv.at[block, pl.ds(first, count), :]
-        return remote(ref, ref, down_send.at[step, piece], down_recv.at[step, piece], "sp", down)
-
-    def arrived_up(step, piece):
-        block = lax.rem(chip - step - 1 + chips, chips)
-        first, count = pieces[piece]
-        ref = kv.at[block, pl.ds(first, count), :]
-        return remote(ref, ref, up_send.at[step, piece], up_recv.at[step, piece], "sp", up)
-
-    def arrived_down(step, piece):
-        block = lax.rem(chip + step + 1, chips)
-        first, count = pieces[piece]
-        ref = kv.at[block, pl.ds(first, count), :]
-        return remote(ref, ref, down_send.at[step, piece], down_recv.at[step, piece], "sp", down)
+    def piece_ref(block, piece):
+        return kv.at[block, pl.ds(*pieces[piece]), :]
+
+    def upward(block, piece):
+        ref = piece_ref(block, piece)
+        return remote(ref, ref, up_send.at[block, piece], up_recv.at[block, piece], "sp", up)
+
+    def downward(block, piece):
+        ref = piece_ref(block, piece)
+        return remote(ref, ref, down_send.at[block, piece], down_recv.at[block, piece], "sp", down)
+
+    def send_on(block, piece):
+        @pl.when(need_up(chip + 1, block))
+        def _():
+            upward(block, piece).start()
+
+    def send_back(block, piece):
+        @pl.when(need_down(below, block))
+        def _():
+            downward(block, piece).start()
 
     kept[0].wait()
     traded[0].wait_recv()
-    upward(0, 0).start()
-    downward(0, 0).start()
+    for piece in range(count // 2):
+        send_on(chip, piece)
+        send_back(chip, piece)
     for i in (1, 2):
         kept[i].wait()
         traded[i].wait_recv()
-    upward(0, 1).start()
-    downward(0, 1).start()
+    for piece in range(count // 2, count):
+        send_on(chip, piece)
+        send_back(chip, piece)
     for i in (3, 4):
         kept[i].wait()
         traded[i].wait_recv()
@@ -303,32 +334,29 @@
         near[rows, :] = share
         carry[rows, :] = whole
 
-    def visit(step, _):
-        for piece in range(2):
-            arrived_up(step, piece).wait_recv()
-
-            @pl.when(step + 1 < up_steps)
+    def visit(k, _):
+        for piece in range(count):
+
+            @pl.when(k < up_count)
             def _():
-                upward(step + 1, piece).start()
-
-            @pl.when(step < down_steps)
+                upward(up_block(k), piece).wait_recv()
+                send_on(up_block(k), piece)
+
+            @pl.when(comes_down(k))
             def _():
-                arrived_down(step, piece).wait_recv()
-
-                @pl.when(step + 1 < down_steps)
-                def _():
-                    downward(step + 1, piece).start()
-
-        @pl.when(chip - step - 1 >= 0)
+                downward(down_block(k), piece).wait_recv()
+                send_back(down_block(k), piece)
+
+        @pl.when(k < up_count)
         def _():
             for i in range(4):
-                rows, share, whole = piece_of(chip - step - 1, i, False)
+                rows, share, whole = piece_of(up_block(k), i, False)
                 near[rows, :] += jnp.exp2(-carry[rows, :]) * share
                 carry[rows, :] += whole
 
-        wrapped = chip + step + 1 - chips
-
-        @pl.when((step < down_steps) & (wrapped >= 0) & (chip - wrapped <= reach))
+        wrapped = down_block(k)
+
+        @pl.when(comes_down(k) & (wrapped < chip) & (chip - wrapped <= reach))
         def _():
             for i in range(4):
                 rows, share, whole = piece_of(wrapped, i, False)
@@ -336,7 +364,7 @@
 
         return 0
 
-    lax.fori_loop(0, up_steps, visit, 0)
+    lax.fori_loop(0, steps, visit, 0)
 
     for h in range(2):
         rows = pl.ds(h * both, both)
@@ -350,6 +378,8 @@
     ]
     for copy in back:
         copy.start()
+    pl.semaphore_wait(known.at[0], 2)
+    tell(1)
     for h in range(2):
         mixed[:, at(core * 256 + h * 128, 128)] = mix[h, at(core * tok), :]
     for copy in back:
@@ -419,6 +449,9 @@
         ).astype(jnp.bfloat16)
     sum_start(waves)
 
+    for level in range(1, levels - 1):
+        pl.semaphore_wait(known.at[level], 2)
+        tell(level + 1)
     sum_middle(waves)
     left, right = sum_end(waves)
     for first, part in ((0, left), (half, right)):
@@ -429,6 +462,8 @@
     value = value.astype(jnp.bfloat16)
     for j in range(4):
         stack[pl.ds(j * rows, rows), :] = value[:, j * quarter : (j + 1) * quarter]
+    pl.semaphore_wait(known.at[levels - 1], 2)
+    pl.semaphore_signal(known.at[levels], inc=1, device_id={"sp": partner}, device_id_type=MESH_ID)
     outgoing[...] = jnp.dot(spread[...], stack[...], preferred_element_type=jnp.float32).astype(jnp.bfloat16)
 
     def offsets(w):
@@ -479,6 +514,7 @@
     own_out = pltpu.make_async_copy(
         reply.at[waves - 1, pl.ds(96, 16), :], returned.at[tile(me), :], self_sem.at[1]
     )
+    pl.semaphore_wait(known.at[levels], 1)
     own_in.start()
 
     def send_all(w, _):
@@ -561,6 +597,21 @@
         def _():
             own_out.start()
 
+    def drain_ring(block, _):
+        for piece in range(count):
+
+            @pl.when((block <= chip) & need_up(chip + 1, block))
+            def _():
+                upward(block, piece).wait_send()
+
+            @pl.when(need_down(below, block))
+            def _():
+                downward(block, piece).wait_send()
+
+        return 0
+
+    lax.fori_loop(0, chips, drain_ring, 0)
+
     def turn(it, _):
         @pl.when(it < waves)
         def _():
@@ -622,18 +673,6 @@
     lax.fori_loop(0, waves + 1, drain, 0)
     for copy in traded + back:
         copy.wait_send()
-
-    def drain_ring(step, _):
-        for piece in range(2):
-            upward(step, piece).wait_send()
-
-            @pl.when(step < down_steps)
-            def _():
-                downward(step, piece).wait_send()
-
-        return 0
-
-    lax.fori_loop(0, up_steps, drain_ring, 0)
 
 
 def layer(
@@ -657,7 +696,6 @@
     doc_rows = 16
     longest = chips * both * 3 // 4
     reach = (longest - 1 + both - 1) // both
-    up_steps = chips // 2
     rows, width = resid.shape
     quarter, half = width // 4, width // 2
     peers = 2 * chips
@@ -684,13 +722,14 @@
             pltpu.VMEM((2 * both, 128), f32),
             pltpu.VMEM((2, both, 128), bf16),
             pltpu.VMEM((tok, 512), bf16),
+            pltpu.SemaphoreType.REGULAR(((chips // 4).bit_length() + 1,)),
             dma((5,)),
             dma((5,)),
             dma((5,)),
-            dma((up_steps, 2)),
-            dma((up_steps, 2)),
-            dma((up_steps, 2)),
-            dma((up_steps, 2)),
+            dma((chips, 2)),
+            dma((chips, 2)),
+            dma((chips, 2)),
+            dma((chips, 2)),
             dma((2,)),
             dma((2,)),
             pltpu.VMEM(w_out.shape, bf16),

time: 137 us -> 136 us (level)
  no operation moved by 1% of the time
where the time goes in v4:
time: 136 us
  Pallas kernels  134 us (99%)
  local copies, waits for them, and re-layouts  1.57 us (1%)
    pallas_call x1, Pallas kernels, layer(): pl.pallas_call(functools.partial(layer_kernel, chips, reach), out_shape=j...  134 us

profile of v4, /device:TPU:33, one launch (start us, length us, event | category | flops | bytes accessed | tf_op | source)
XLA Modules:
  0.0 135.6 jit_solution(13345596473451453903)
XLA Ops:
  0.0 134.0 %layer.1 = bf16[32,2048]{1,0:T(8,128)(2,1)} custom-call(bf16[128,512]{1,0:T(8,128)(2,1)} %q_ref.1, bf16[128,256]{1,0:T(8,128)(2,1)} %k_ref.1, bf16[128,256]{1,0:T(8,128)(2,1)} %v_ref.1, bf16[512,2048]{1,0:T(8,128)(2,1)} %w_out_hbm.1, bf16[32,2048]{1,0:T(8,128)(2,1)} %resid_hbm.1, bf16[1,2048,768]{2,1,0:T(8,128)(2,1)} %w_gate_hbm.1, ...), custom_call_target="tpu_custom_call" | custom-call | tf_op jit(solution)/shard_map/layer/pallas_call | solution.py:709
  134.0 1.6 %copy.15 = bf16[32,2048]{1,0:T(8,128)(2,1)} copy(bf16[32,2048]{1,0:T(8,128)(2,1)} %layer.1) | data formatting | bytes 262144
